TPU v7x, 256 devices: a whole 4x4x8 slice. The times are simulated.
256 devices in a mesh: sp: 64 (over z, x, core), tp: 4 (over y).
Axes of the slice: x: 4, y: 4, z: 8, core: 2. Of those that a mesh axis runs over, the one named last changes fastest.
Arguments:
- stream: bfloat16 [16384, 2048], P('sp'), may hold values from -6 to 6
- query: bfloat16 [16384, 1024], P('sp', 'tp'), may hold values from -6 to 6
- forget_gate_logits: bfloat16 [16384, 1024], P('sp', 'tp'), may hold values from -4 to 4
- value_input_rows: bfloat16 [16384, 1024], P('sp', 'tp'), may hold values from -6 to 6
- output_gate_logits: bfloat16 [16384, 1024], P('sp', 'tp'), may hold values from -6 to 6
- forget_floor_margin: float32 [8, 128], P('tp'), as said below
- additional_fading_speed: float32 [16384, 8], P('sp', 'tp'), may hold values from -0.7 to 0, as said below
- head_norm_gain: float32 [128], replicated, may hold values from 0.1 to 1.9
- output_head_weight: bfloat16 [1024, 2048], replicated, may hold values from -0.1875 to 0.1875
- feedforward_norm_gain: float32 [2048], replicated, may hold values from 0.1 to 1.9
- selected_expert_index: int32 [16384, 2], P('sp'), may hold values from 0 to 63, all different within a row; in each aligned block of 64 rows (0 to 63, 64 to 127, ...) at most 4 rows name the same one
- selected_expert_weight: float32 [16384, 2], P(('sp', 'tp')), may hold values from 0.2 to 1
- expert_gate_weight: bfloat16 [64, 2048, 1024], P('sp', None, 'tp'), may hold values from -0.125 to 0.125
- expert_up_weight: bfloat16 [64, 2048, 1024], P('sp', None, 'tp'), may hold values from -0.125 to 0.125
- expert_down_weight: bfloat16 [64, 1024, 2048], P('sp', 'tp'), may hold values from -0.1875 to 0.1875
Outputs:
- layer_out: bfloat16 [16384, 2048], P(('sp', 'tp'))
Inputs may be any that keep to these rules, and one draw needn't show every extreme that they name: `forget_floor_margin`: positive. `additional_fading_speed`: zero at most positions. `selected_expert_index`: the 2 experts of a position differ; in each aligned block of 64 positions no expert is named more than 4 times, and in every draw some expert is named exactly 4 times in some block.
All inputs are finite; a program needn't handle non-finite values.
Results may differ from a plain program's by a relative error of at most 0.006.
Values may be sent and summed in bfloat16 or wider, within the bound.
A program may use at most 64 MiB of HBM per device.

v0:
```python
import jax
import jax.numpy as jnp
from jax import lax
from jax.sharding import Mesh
from jax.sharding import PartitionSpec as P

BLOCK = 64
SP = ("sp_0", "sp_1", "sp_2")
SP_TP = ("sp_0", "sp_1", "sp_2", "tp")


EPS = 1e-06
HIGH = lax.Precision.HIGHEST


def filled_with(value, identity):
    return jax.tree.map(
        lambda part, zero: jnp.zeros_like(part) + jnp.asarray(zero, part.dtype), value, identity
    )


def carried_in(value, axes, combine, identity):
    before = start = filled_with(value, identity)
    subtotal = value
    for axis in reversed(axes):
        peers, index = (lax.axis_size(axis), lax.axis_index(axis))
        pieces = jax.tree.map(lambda part: lax.all_gather(part, axis), subtotal)
        inside, subtotal = (start, start)
        for k in range(peers):
            passed = k < index
            subtotal = combine(subtotal, jax.tree.map(lambda part: part[k], pieces))
            inside = jax.tree.map(lambda new, old: jnp.where(passed, new, old), subtotal, inside)
        before = combine(inside, before)
    return before


def laid_out(blocks, dim):
    blocks = jnp.moveaxis(blocks, 0, dim)
    lengths = blocks.shape
    return blocks.reshape(*lengths[:dim], lengths[dim] * lengths[dim + 1], *lengths[dim + 2 :])


def on_gathered_pieces(value, axis, dim, work, out_dim):
    span = value.shape[dim]
    pieces = jnp.split(value, 2, axis=dim) if span % 2 == 0 else [value]
    first = jnp.arange(lax.axis_size(axis)) * span
    blocks = [lax.all_gather(share, axis) for share in pieces]
    made = [jax.vmap(work)(b, first + k * (span // len(pieces))) for k, b in enumerate(blocks)]
    return laid_out(jnp.concatenate(made, axis=out_dim + 1), out_dim)


def cut_to_segments(array, segment_span, heads):
    width = array.shape[1] // heads
    shaped = array.astype(jnp.float32).reshape(
        array.shape[0] // segment_span, segment_span, heads, width
    )
    return jnp.transpose(shaped, (0, 2, 1, 3))


def slot_ranks(chosen, experts):
    onehot = (chosen[:, :, None] == jnp.arange(experts, dtype=jnp.int32)[None, None, :]).astype(
        jnp.int32
    )
    earlier = jnp.cumsum(onehot, axis=1) - onehot
    return jnp.sum(earlier * onehot, axis=2)


def expert_hidden(rows, w_gate, w_up):
    flat = rows.reshape(-1, rows.shape[-1])
    gate_part = jnp.dot(flat, w_gate, preferred_element_type=jnp.float32)
    up_part = jnp.dot(flat, w_up, preferred_element_type=jnp.float32)
    hidden = (jax.nn.silu(gate_part) * up_part).astype(jnp.bfloat16)
    return hidden.reshape(rows.shape[:-1] + (w_gate.shape[1],))


def chain_combine(earlier, later):
    return (earlier[0] * later[0], later[0][..., None] * earlier[1] + later[1])


def carry_step(state, pieces):
    return (jnp.exp(pieces[1])[..., None] * state + pieces[0], state)


def per_device(
    stream,
    query,
    forget_gate_logits,
    value_input_rows,
    output_gate_logits,
    forget_floor_margin,
    additional_fading_speed,
    head_norm_gain,
    output_head_weight,
    feedforward_norm_gain,
    selected_expert_index,
    selected_expert_weight,
    expert_gate_weight,
    expert_up_weight,
    expert_down_weight,
):
    f32 = jnp.float32
    tok_rows, model_width = stream.shape
    local_scan_lanes, head_dim = forget_floor_margin.shape
    segment_span = BLOCK
    tp_count = lax.axis_size("tp")
    tp_rank = lax.axis_index("tp")
    query_blk = cut_to_segments(query, segment_span, local_scan_lanes)
    scores_segment_slice = cut_to_segments(forget_gate_logits, segment_span, local_scan_lanes)
    value_blk = cut_to_segments(value_input_rows, segment_span, local_scan_lanes)
    spike_segment_slice = cut_to_segments(additional_fading_speed, segment_span, local_scan_lanes)
    clearance_amount = forget_floor_margin[None, :, None, :]
    logarithmic_fading_speed = (
        jnp.logaddexp(
            jnp.log1p(-clearance_amount),
            jnp.log(clearance_amount) + jax.nn.log_sigmoid(scores_segment_slice),
        )
        + spike_segment_slice
    )
    key_in = clearance_amount * jax.nn.sigmoid(-scores_segment_slice)
    cumul = jnp.cumsum(logarithmic_fading_speed, axis=2)
    last = cumul[:, :, -1:, :]
    causal = jnp.tril(jnp.ones((segment_span, segment_span), dtype=bool))[:, :, None]
    pair_log = cumul[:, :, :, None, :] - cumul[:, :, None, :, :]
    decay = jnp.exp(jnp.where(causal, pair_log, -jnp.inf))
    scores = jnp.sum(query_blk[:, :, :, None, :] * key_in[:, :, None, :, :] * decay, axis=-1)
    inner = jnp.einsum("bhts,bhse->bhte", scores, value_blk, precision=HIGH)
    block_state = jnp.einsum(
        "bhsd,bhse->bhde", key_in * jnp.exp(last - cumul), value_blk, precision=HIGH
    )
    block_last = last[:, :, 0, :]
    last_cumul = jnp.cumsum(block_last, axis=0)
    device_decay = jnp.exp(last_cumul[-1])
    zero_state = jnp.zeros(block_state.shape[1:], f32)
    local_final, local_starts = lax.scan(carry_step, zero_state, (block_state, block_last))
    carried = carried_in(
        (device_decay, local_final), SP, chain_combine, (jnp.ones_like(device_decay), zero_state)
    )
    incoming = carried[1]
    before = (last_cumul - block_last)[:, :, None, :]
    recur = inner + jnp.einsum(
        "bhtd,bhde->bhte", query_blk * jnp.exp(cumul), local_starts, precision=HIGH
    )
    recur = recur + jnp.einsum(
        "bhtd,hde->bhte", query_blk * jnp.exp(before + cumul), incoming, precision=HIGH
    )
    recur = jnp.transpose(recur, (0, 2, 1, 3)).reshape(tok_rows, local_scan_lanes, head_dim)
    scale = lax.rsqrt(jnp.mean(recur * recur, axis=-1, keepdims=True) + EPS)
    gate_in = output_gate_logits.astype(f32).reshape(tok_rows, local_scan_lanes, head_dim)
    gated = (
        (recur * scale * head_norm_gain * jax.nn.silu(gate_in))
        .astype(jnp.bfloat16)
        .reshape(tok_rows, local_scan_lanes * head_dim)
    )
    projected = jnp.dot(
        lax.all_gather(gated, "tp", axis=1, tiled=True),
        output_head_weight,
        preferred_element_type=f32,
    )
    mixed = (stream.astype(f32) + projected).astype(jnp.bfloat16)
    mixed_wide = lax.optimization_barrier(mixed).astype(f32)
    normed = (
        mixed_wide
        * lax.rsqrt(jnp.mean(mixed_wide * mixed_wide, axis=-1, keepdims=True) + EPS)
        * feedforward_norm_gain
    ).astype(jnp.bfloat16)
    topk = selected_expert_index.shape[1]
    experts = lax.axis_size(SP) * expert_gate_weight.shape[0]
    group_rows = tok_rows // tp_count
    cap = 2 * topk * group_rows // experts
    assigned = group_rows * topk
    w_gate = expert_gate_weight[0]
    w_up = expert_up_weight[0]
    w_down = expert_down_weight[0]
    own_route = lax.dynamic_slice_in_dim(selected_expert_index, tp_rank * group_rows, group_rows, 0)
    own_ranks = slot_ranks(own_route.reshape(1, -1), experts)[0]
    padded = jnp.concatenate([normed, jnp.zeros((1, model_width), jnp.bfloat16)], axis=0)
    dest = own_route.reshape(-1) * cap + own_ranks
    owner = tp_rank * group_rows + jnp.arange(assigned, dtype=jnp.int32) // topk
    table = jnp.full((experts * cap,), tok_rows, jnp.int32).at[dest].set(owner)
    outgoing = padded[table].reshape(1, experts, cap, model_width)
    arrived = lax.all_to_all(outgoing, SP, split_axis=1, concat_axis=1, tiled=True)

    def hidden_piece(piece, start):
        return expert_hidden(piece, w_gate, w_up)

    hidden = on_gathered_pieces(arrived, "tp", 0, hidden_piece, 0)
    hidden_flat = hidden.reshape(-1, hidden.shape[-1])
    summed = lax.psum_scatter(
        jnp.dot(hidden_flat, w_down, preferred_element_type=f32),
        "tp",
        scatter_dimension=0,
        tiled=True,
    )
    expert_out = summed.astype(jnp.bfloat16).reshape(experts, cap, model_width)
    returned = lax.all_to_all(expert_out, SP, split_axis=0, concat_axis=0, tiled=True)
    index = own_route.reshape(-1) * cap + own_ranks
    picked = (
        returned.reshape(-1, model_width)[index].astype(f32).reshape(group_rows, topk, model_width)
    )
    routed = jnp.sum(picked * selected_expert_weight[:, :, None], axis=1)
    own_mixed = lax.dynamic_slice_in_dim(mixed_wide, tp_rank * group_rows, group_rows, 0)
    return (own_mixed + routed).astype(jnp.bfloat16)


def solution(mesh):
    finer = Mesh(mesh.devices.reshape(8, 4, 2, mesh.shape["tp"]), ("sp_0", "sp_1", "sp_2", "tp"))
    in_specs = (
        P(SP, None),
        P(SP, "tp"),
        P(SP, "tp"),
        P(SP, "tp"),
        P(SP, "tp"),
        P("tp", None),
        P(SP, "tp"),
        P(),
        P(),
        P(),
        P(SP, None),
        P(SP_TP, None),
        P(SP, None, "tp"),
        P(SP, None, "tp"),
        P(SP, "tp", None),
    )
    out_specs = P(SP_TP, None)
    return jax.shard_map(
        per_device, mesh=finer, in_specs=in_specs, out_specs=out_specs, check_vma=False
    )
```

profile of v0, /device:TPU:1, one launch (start us, length us, event | category | flops | bytes accessed | tf_op | source)
XLA Modules:
  0.0 353.9 jit_solution(268023712368840436)
XLA Ops:
  6.5 1.1 fusion.10
  9.8 4.7 %all_gather.35 = f32[2,2,128]{2,1,0:T(2,128)S(1)} all-gather(f32[1,2,128]{2,1,0:T(2,128)S(1)} %slice_exponential_fusion), channel_id=1, replica_groups=mesh['sp_0'=8,'sp_1'=4,'sp_2'=2,'tp'=4] {'sp_2'}, dimensions={0}, use_global_device_ids=true | all-gather | bytes 3072 | tf_op jit(solution)/shard_map/all_gather | solution.py:27
  14.5 6.0 %all_gather.36 = f32[4,2,128]{2,1,0:T(2,128)S(1)} all-gather(f32[1,2,128]{2,1,0:T(2,128)S(1)} %get-tuple-element.83), channel_id=1, replica_groups=mesh['sp_0'=8,'sp_1'=4,'sp_2'=2,'tp'=4] {'sp_1'}, dimensions={0}, use_global_device_ids=true | all-gather | bytes 5120 | tf_op jit(solution)/shard_map/all_gather | solution.py:27
  20.5 1.0 reshape.287
  22.7 1.4 fusion.22
  25.5 4.0 %all-gather = f32[4,128,128]{2,1,0:T(8,128)S(1)} all-gather(f32[2,128,128]{2,1,0:T(8,128)S(1)} %get-tuple-element.34), channel_id=2, replica_groups=mesh['sp_0'=8,'sp_1'=4,'sp_2'=2,'tp'=4] {'sp_2'}, dimensions={0}, use_global_device_ids=true | all-gather | bytes 393216 | tf_op jit(solution)/shard_map/all_gather | solution.py:27
  29.6 9.9 %all_gather.40 = f32[4,2,128,128]{3,2,1,0:T(8,128)S(1)} all-gather(f32[1,2,128,128]{3,2,1,0:T(8,128)S(1)} %bitcast_add_fusion.5), channel_id=1, replica_groups=mesh['sp_0'=8,'sp_1'=4,'sp_2'=2,'tp'=4] {'sp_1'}, dimensions={0}, use_global_device_ids=true | all-gather | bytes 655360 | tf_op jit(solution)/shard_map/all_gather | solution.py:27
  42.5 15.4 %all_gather.37 = f32[8,2,128]{2,1,0:T(2,128)S(1)} all-gather(f32[1,2,128]{2,1,0:T(2,128)S(1)} %get-tuple-element.77), channel_id=1, replica_groups=mesh['sp_0'=8,'sp_1'=4,'sp_2'=2,'tp'=4] {'sp_0'}, dimensions={0}, use_global_device_ids=true | all-gather | bytes 9216 | tf_op jit(solution)/shard_map/all_gather | solution.py:27
  58.0 6.4 %multiply_reduce_fusion = f32[4,2,64,64]{3,2,1,0:T(8,128)S(1)} fusion(f32[4,2,64,128]{3,2,1,0:T(8,128)S(1)} %reduce_window_sum.35, f32[4,2,64,128]{3,2,1,0:T(8,128)S(1)} %get-tuple-element.89, f32[4,2,64,128]{3,2,1,0:T(8,128)} %get-tuple-element.90, pred[64,64]{1,0:T(8,128)(4,1)S(1)} %iota_compare_fusion.1), kind=kLoop, calls=%fused_computation.6 | loop fusion | flops 20938752 | bytes 921600 | tf_op jit(solution)/shard_map/reduce_sum | solution.py:125
  64.7 1.3 fusion.3
  66.0 12.6 %all-gather.5.cloned.1.call-done = f32[8,2,128,128]{3,2,1,0:T(8,128)} async-done(((f32[1,2,128,128]{3,2,1,0:T(8,128)}), f32[8,2,128,128]{3,2,1,0:T(8,128)}) %all-gather.5.cloned.1.call-update) | async-done | bytes 1048592 | tf_op jit(solution)/shard_map/all_gather | solution.py:27
  78.5 2.4 multiply_reduce_fusion.3
  81.8 10.3 %all_gather.42 = bf16[256,1024]{1,0:T(8,128)(2,1)S(1)} all-gather(bf16[256,256]{1,0:T(8,128)(2,1)S(1)} %fusion.32), channel_id=1, replica_groups=mesh['sp_0'=8,'sp_1'=4,'sp_2'=2,'tp'=4] {'tp'}, dimensions={1}, use_global_device_ids=true | all-gather | bytes 655360 | tf_op jit(solution)/shard_map/all_gather | solution.py:155
  92.1 3.8 %fusion = bf16[256,2048]{1,0:T(8,128)(2,1)S(1)} fusion(bf16[256,1024]{1,0:T(8,128)(2,1)S(1)} %all_gather.42, bf16[1024,2048]{1,0:T(8,128)(2,1)} %param.25, bf16[256,2048]{1,0:T(8,128)(2,1)} %param.17), kind=kOutput, calls=%fused_computation.8 | convolution fusion | flops 1075314688 | bytes 6815744 | tf_op jit(solution)/shard_map/dot_general | solution.py:154
  96.5 2.3 gather_fusion
  98.9 1.5 reshape.281
  100.3 43.7 %all_to_all.10 = bf16[1,64,4,2048]{3,2,0,1:T(4,128)(2,1)S(1)} all-to-all(bf16[1,64,4,2048]{3,2,0,1:T(4,128)(2,1)S(1)} %bitcast.287), channel_id=1, replica_groups=mesh['sp_0'=8,'sp_1'=4,'sp_2'=2,'tp'=4] {'sp_0','sp_1','sp_2'}, dimensions={1} | all-to-all | bytes 2097152 | tf_op jit(solution)/shard_map/all_to_all | solution.py:181
  144.0 1.5 copy.86
  145.6 47.0 %all-gather.7.cloned.1.call-done = bf16[4,64,4,2048]{3,1,2,0:T(8,128)(2,1)} async-done(((bf16[1,64,4,2048]{3,1,2,0:T(8,128)(2,1)}), bf16[4,64,4,2048]{3,1,2,0:T(8,128)(2,1)}) %all-gather.7.cloned.1.call-update) | async-done | bytes 4194320 | tf_op jit(solution)/shard_map/all_gather | solution.py:47
  192.7 7.4 %copy.87 = bf16[4,64,4,2048]{3,2,1,0:T(4,128)(2,1)} copy(bf16[4,64,4,2048]{3,1,2,0:T(8,128)(2,1)} %all-gather.7.cloned.1.call-done) | data formatting | bytes 8388608 | tf_op jit(solution)/shard_map/all_gather | solution.py:47
  200.1 7.0 %reshape.282 = bf16[4,256,2048]{2,1,0:T(8,128)(2,1)} reshape(bf16[4,64,4,2048]{3,2,1,0:T(4,128)(2,1)} %copy.87) | data formatting | bytes 8388608 | tf_op jit(solution)/shard_map/vmap()/reshape | solution.py:69
  207.1 3.6 %fusion.7 = f32[4,256,256]{2,1,0:T(8,128)S(1)} fusion(bf16[4,256,2048]{2,1,0:T(8,128)(2,1)} %reshape.282, bf16[1,2048,256]{2,1,0:T(8,128)(2,1)S(1)} %copy-done.6), kind=kOutput, calls=%fused_computation.20 | convolution fusion | flops 1073741824 | bytes 6291456 | tf_op jit(solution)/shard_map/vmap()/dot_general | solution.py:70
  210.8 1.3 fusion.1
  212.1 4.5 %fusion.4 = f32[1024,2048]{1,0:T(8,128)} fusion(bf16[1024,256]{1,0:T(8,128)(2,1)S(1)} %bitcast.290, bf16[1,256,2048]{2,1,0:T(8,128)(2,1)S(1)} %copy-done), kind=kOutput, calls=%fused_computation.17 | convolution fusion | flops 1073741824 | bytes 9961472 | tf_op jit(solution)/shard_map/dot_general | solution.py:189
  216.6 83.7 %reduce-scatter.2.cloned.1.call-done = f32[256,2048]{1,0:T(8,128)} async-done(((f32[1024,2048]{1,0:T(8,128)}), f32[256,2048]{1,0:T(8,128)}) %reduce-scatter.2.cloned.1.call-update) | async-done | bytes 2097168 | tf_op jit(solution)/shard_map/reduce_scatter | solution.py:188
  300.3 1.7 convert_element_type.64
  302.1 1.2 reshape.284
  303.3 10.7 %all-to-all-start.1 = ((bf16[64,4,2048]{2,1,0:T(4,128)(2,1)}), bf16[64,4,2048]{2,1,0:T(4,128)(2,1)S(1)}, u32[]{:S(2)}, u32[]{:S(2)}) async-start(bf16[64,4,2048]{2,1,0:T(4,128)(2,1)} %reshape.284), calls=%async_computation.2 | async-start | bytes 2097152 | tf_op jit(solution)/shard_map/all_to_all | solution.py:195
  314.1 1.6 convert_element_type.60
  315.7 26.5 %all-to-all-done.1 = bf16[64,4,2048]{2,1,0:T(4,128)(2,1)S(1)} async-done(((bf16[64,4,2048]{2,1,0:T(4,128)(2,1)}), bf16[64,4,2048]{2,1,0:T(4,128)(2,1)S(1)}, u32[]{:S(2)}, u32[]{:S(2)}) %all-to-all-start.1) | async-done | bytes 1048608 | tf_op jit(solution)/shard_map/all_to_all | solution.py:195
  344.0 1.5 multiply_reduce_fusion.2
  345.6 1.8 add_convert_fusion
  (88 shorter events, 12.2 us)
Async XLA Ops:
  6.5 205.6 %copy-start = (bf16[1,256,2048]{2,1,0:T(8,128)(2,1)S(1)}, bf16[1,256,2048]{2,1,0:T(8,128)(2,1)}, u32[]{:S(2)}) copy-start(bf16[1,256,2048]{2,1,0:T(8,128)(2,1)} %param.31) | copy-start | bytes 3145732
  6.5 72.0 %all-gather.5.cloned.1.call-start = ((), (), s32[]{:S(2)}) async-start(), calls=%async_computation.3 | async-start | bytes 1179648 | tf_op jit(solution)/shard_map/all_gather | solution.py:27
  21.7 18.8 %copy-start.8 = (f32[128]{0:T(128)S(1)}, f32[128]{0:T(128)}, u32[]{:S(2)}) copy-start(f32[128]{0:T(128)} %param.24) | copy-start | bytes 1540
  21.7 18.8 %copy-start.5 = (s32[256,2]{0,1:T(2,128)S(1)}, s32[256,2]{0,1:T(2,128)}, u32[]{:S(2)}) copy-start(s32[256,2]{0,1:T(2,128)} %param.27) | copy-start | bytes 6148
  40.4 152.3 %all-gather.7.cloned.1.call-start = ((), (), s32[]{:S(2)}) async-start(), calls=%async_computation.5 | async-start | bytes 5242880 | tf_op jit(solution)/shard_map/all_gather | solution.py:47
  64.4 17.3 %copy-start.2 = (bf16[256,256]{1,0:T(8,128)(2,1)S(1)}, bf16[256,256]{1,0:T(8,128)(2,1)}, u32[]{:S(2)}) copy-start(bf16[256,256]{1,0:T(8,128)(2,1)} %param.21) | copy-start | bytes 393220
  92.1 4.1 %copy-start.3 = (f32[2048]{0:T(1024)S(1)}, f32[2048]{0:T(1024)}, u32[]{:S(2)}) copy-start(f32[2048]{0:T(1024)} %param.26) | copy-start | bytes 24580
  145.6 154.7 %reduce-scatter.2.cloned.1.call-start = ((), (), s32[]{:S(2)}) async-start(), calls=%async_computation.4 | async-start | bytes 10485760 | tf_op jit(solution)/shard_map/reduce_scatter | solution.py:188
  200.1 7.0 %copy-start.6 = (bf16[1,2048,256]{2,1,0:T(8,128)(2,1)S(1)}, bf16[1,2048,256]{2,1,0:T(8,128)(2,1)}, u32[]{:S(2)}) copy-start(bf16[1,2048,256]{2,1,0:T(8,128)(2,1)} %param.29) | copy-start | bytes 3145732
  207.1 3.6 %copy-start.1 = (bf16[4,256,2048]{2,1,0:T(8,128)(2,1)S(1)}, bf16[4,256,2048]{2,1,0:T(8,128)(2,1)}, u32[]{:S(2)}) copy-start(bf16[4,256,2048]{2,1,0:T(8,128)(2,1)} %reshape.282) | copy-start | bytes 12582916
  207.1 3.7 %copy-start.7 = (bf16[1,2048,256]{2,1,0:T(8,128)(2,1)S(1)}, bf16[1,2048,256]{2,1,0:T(8,128)(2,1)}, u32[]{:S(2)}) copy-start(bf16[1,2048,256]{2,1,0:T(8,128)(2,1)} %param.30) | copy-start | bytes 3145732
  216.6 97.4 %copy-start.4 = (f32[64,2]{0,1:T(2,128)S(1)}, f32[64,2]{0,1:T(2,128)}, u32[]{:S(2)}) copy-start(f32[64,2]{0,1:T(2,128)} %param.28) | copy-start | bytes 1540
  303.3 38.9 %all-to-all-start.1 = ((bf16[64,4,2048]{2,1,0:T(4,128)(2,1)}), bf16[64,4,2048]{2,1,0:T(4,128)(2,1)S(1)}, u32[]{:S(2)}, u32[]{:S(2)}) async-start(bf16[64,4,2048]{2,1,0:T(4,128)(2,1)} %reshape.284), calls=%async_computation.2 | async-start | bytes 2097152 | tf_op jit(solution)/shard_map/all_to_all | solution.py:195
Sparse Core Ops, SparseCore 0:
  40.5 37.9 all-gather.4
  145.7 46.9 all-gather.6
  216.7 83.5 reduce-scatter.1
where the time goes:
time: 355 us; the launch traced here: 354 us
  waiting for transfers between devices  170 us (48%)
  blocking collectives  94 us (26%)
  local copies, waits for them, and re-layouts  28.3 us (8%)
  other arithmetic  19.7 us (6%)
  matrix products  17.7 us (5%)
  between operations  13.5 us (4%)
  starting transfers between devices  10.8 us (3%)
    reduce_scatter x1, waiting for transfers between devices, per_device(): lax.psum_scatter(jnp.dot(hidden_flat, w_down, preferred_element_type=f32)...  83.7 us
    all_gather x1, waiting for transfers between devices, on_gathered_pieces(): blocks = [lax.all_gather(share, axis) for share in pieces]  47 us
    all_to_all x1, blocking collectives, per_device(): lax.all_to_all(outgoing, SP, split_axis=1, concat_axis=1, tiled=True)  43.7 us
    all_gather x5, blocking collectives, carried_in(): pieces = jax.tree.map(lambda part: lax.all_gather(part, axis), subtotal)  40 us
    all_to_all x1, waiting for transfers between devices, per_device(): lax.all_to_all(expert_out, SP, split_axis=0, concat_axis=0, tiled=True)  26.5 us
    all_gather x1, waiting for transfers between devices, carried_in(): pieces = jax.tree.map(lambda part: lax.all_gather(part, axis), subtotal)  12.6 us
    all_to_all x1, starting transfers between devices, per_device(): lax.all_to_all(expert_out, SP, split_axis=0, concat_axis=0, tiled=True)  10.7 us
    all_gather x1, blocking collectives, per_device(): lax.all_gather(gated, 'tp', axis=1, tiled=True)  10.3 us
  transfers between devices with their start and end apart: 4, of which 4 were waited for; matrix products, arithmetic and copies ran while one was open for 3% of the time, Pallas kernels for 0%

commit v1 on v0

v1 whole, which is shorter than its diff:
```python
import functools

import jax
import jax.numpy as jnp
from jax import lax
from jax.experimental import pallas as pl
from jax.experimental.pallas import tpu as pltpu
from jax.sharding import Mesh
from jax.sharding import PartitionSpec as P

SP = ("sp_0", "sp_1", "sp_2")
SP_TP = ("sp_0", "sp_1", "sp_2", "tp")
EPS = 1e-06
f32 = jnp.float32
bf16 = jnp.bfloat16
NZ, NX, NC, NY = 8, 4, 2, 4
ROWS = 256
GROUP = 64
CAP = 4
NT = (((1,), (1,)), ((), ()))


def dot(a, b):
    return jnp.dot(a, b, preferred_element_type=f32)


def dot_nt(a, b):
    return lax.dot_general(a, b, NT, preferred_element_type=f32)


def split2(x):
    high = x.astype(bf16)
    return high, (x - high.astype(f32)).astype(bf16)


def split3(x):
    high = x.astype(bf16)
    rest = x - high.astype(f32)
    mid = rest.astype(bf16)
    return high, mid, (rest - mid.astype(f32)).astype(bf16)


def product_nt(a, b):
    ah, al = split2(a)
    bh, bl = split2(b)
    return dot_nt(jnp.concatenate([ah, ah, al], axis=1), jnp.concatenate([bh, bl, bh], axis=1))


def ring_step(n):
    return (NZ + ((n + 1) // 2) * (1 - 2 * ((n + 1) % 2))) % NZ


def remote(src, dst, send_sem, recv_sem, device):
    return pltpu.make_async_remote_copy(
        src_ref=src,
        dst_ref=dst,
        send_sem=send_sem,
        recv_sem=recv_sem,
        device_id=device,
        device_id_type=pl.DeviceIdType.MESH,
    )


def take(ref, sem):
    pltpu.make_async_copy(ref, ref, sem).wait()


def kernel(
    dest_ref, base_ref, wsel_ref, mar_ref, fade_ref, hg_ref, fg_ref,
    q_hbm, f_hbm, v_hbm, og_hbm, stream_hbm, wh_hbm, wg_hbm, wu_hbm, wd_hbm,
    out_ref,
    qb, fb, vb, ob, stream, wh, wg, wu, wd,
    rec, qend, st_send, st_recv, tq, xr, px, us, zr, isend, inc,
    gall, acc, mixed, normed, sbuf, xbuf, hsend, hrec, rsend, rbuf, picks,
    load_sem, s_sem, c_sem, gm, gp, gr, wm, wp, wr, xs, yfm, yfp, yrm, yrp, hs, rs,
):
    z, x, c, p = [lax.axis_index(name) for name in SP_TP]
    up, down, far = (p + 1) % NY, (p + NY - 1) % NY, (p + 2) % NY
    at_up, at_down = {"tp": up}, {"tp": down}

    loads = [
        pltpu.make_async_copy(src, dst, load_sem.at[k])
        for k, (src, dst) in enumerate(
            [
                (f_hbm, fb), (q_hbm, qb), (v_hbm, vb), (wd_hbm, wd.at[p]), (og_hbm, ob),
                (wh_hbm, wh), (stream_hbm, stream), (wg_hbm, wg), (wu_hbm, wu),
            ]
        )
    ]
    for load in loads:
        load.start()

    barrier = pltpu.get_barrier_semaphore()

    def greet(k, _):
        dz, dx, dc = k // 8, (k // 2) % 4, k % 2
        pl.semaphore_signal(
            barrier,
            inc=1,
            device_id={"sp_0": (z + dz) % NZ, "sp_1": (x + dx) % NX, "sp_2": (c + dc) % NC},
            device_id_type=pl.DeviceIdType.MESH,
        )
        return 0

    lax.fori_loop(1, NZ * NX * NC, greet, 0)
    for peer in (up, down, far):
        pl.semaphore_signal(
            barrier, inc=1, device_id={"tp": peer}, device_id_type=pl.DeviceIdType.MESH
        )

    row = lax.broadcasted_iota(jnp.int32, (ROWS, ROWS), 0)
    col = lax.broadcasted_iota(jnp.int32, (ROWS, ROWS), 1)

    def ones_where(condition):
        return jnp.where(condition, 1.0, 0.0).astype(bf16)

    def level_sum(shift):
        odd = ((row >> shift) & 1) == 1
        same = (row >> shift) == (col >> shift)
        return ones_where(same & ((odd & (col <= row)) | (jnp.logical_not(odd) & (col > row))))

    loads[0].wait()
    margin = mar_ref[...]
    keys = margin * jax.nn.sigmoid(-fb[...].astype(f32))
    fade = fade_ref[...]
    fades = jnp.concatenate(
        [jnp.broadcast_to(fade[:, h : h + 1], (ROWS, 128)) for h in range(2)], axis=1
    )
    log_decay = jnp.log1p(-keys) + fades
    parts = jnp.concatenate(split3(log_decay), axis=1)

    def sums(matrix):
        three = dot(matrix, parts)
        return three[:, 0:256] + (three[:, 256:512] + three[:, 512:768])

    loads[1].wait()
    loads[2].wait()
    queries = qb[...].astype(f32)
    to_start = sums(ones_where(col <= row))
    to_end = sums(ones_where(col > row))
    qend[...] = queries * jnp.exp(to_start)
    kend = keys * jnp.exp(to_end)
    total = jnp.exp(to_start[ROWS - 1 : ROWS, :])
    vt = jnp.transpose(vb[...].astype(f32), (1, 0)).astype(bf16)
    for h in range(2):
        lanes = slice(128 * h, 128 * (h + 1))
        kh, kl = split2(kend[:, lanes])
        both = dot(vt[lanes, :], jnp.concatenate([kh, kl], axis=1))
        st_send[h, 0:128, :] = both[:, 0:128] + both[:, 128:256]
        st_send[h, 128:136, :] = jnp.broadcast_to(total[:, lanes], (8, 128))

    pl.semaphore_wait(barrier, NZ * NX * NC - 1 + 3)

    to_core = remote(st_send, st_recv, s_sem.at[0], c_sem.at[0], {"sp_2": 1 - c})
    to_core.start()
    loads[3].wait()
    for half in range(2):
        rows = pl.ds(128 * half, 128)
        other = pl.ds(128 * (1 - half), 128)
        remote(wd.at[p, rows], wd.at[p, rows], s_sem.at[1], wm.at[half], at_up).start()
        remote(wd.at[p, other], wd.at[p, other], s_sem.at[1], wp.at[1 - half], at_down).start()

    def inside(h):
        lanes = slice(128 * h, 128 * (h + 1))
        qh, kh = queries[:, lanes], keys[:, lanes]
        exponent = sums_of[3][:, lanes]
        odd = ((row[:, 0:128] >> 3) & 1) == 1
        exponent = jnp.where(odd, exponent, -exponent)
        scores = product_nt(qh * jnp.exp(exponent), kh * jnp.exp(-exponent))
        scores = jnp.where(((row >> 4) == (col >> 4)) & (col <= row), scores, 0.0)
        for shift in (4, 5, 6, 7):
            weight = jnp.exp(sums_of[shift][:, lanes])
            odd = ((row[:, 0:128] >> shift) & 1) == 1
            part = product_nt(jnp.where(odd, qh * weight, 0.0), jnp.where(odd, 0.0, kh * weight))
            scores = scores + jnp.where((row >> (shift + 1)) == (col >> (shift + 1)), part, 0.0)
        sh, sl = split2(scores)
        vh = vb[:, lanes]
        rec[h] = dot(sh, vh) + dot(sl, vh)

    take(st_recv, c_sem.at[0])
    cf = c.astype(f32)
    own, other = st_send[c], st_recv[c]
    first = own * (1.0 - cf) + other * cf
    second = other * (1.0 - cf) + own * cf
    chip_state = second[128:129, :] * first[0:128, :] + second[0:128, :]
    chip_decay = first[128:136, :] * second[128:136, :]
    for k in range(NX):
        tq[k, 0:32, :] = chip_state[32 * k : 32 * (k + 1), :]
        tq[k, 32:40, :] = chip_decay
    for dx in range(1, NX):
        to = (x + dx) % NX
        remote(tq.at[to], xr.at[x], s_sem.at[2], c_sem.at[1], {"sp_1": to}).start()
    xr[x] = tq[x]
    sums_of = {shift: sums(level_sum(shift)) for shift in (3, 4, 5, 6, 7)}
    take(xr.at[pl.ds(0, NX - 1)], c_sem.at[1])
    state, decay = jnp.zeros((32, 128), f32), jnp.ones((8, 128), f32)
    for k in range(NX):
        px[k, 0:32, :] = state
        px[k, 32:40, :] = decay
        state = xr[k, 32:33, :] * state + xr[k, 0:32, :]
        decay = xr[k, 32:40, :] * decay
    us[0:32, :] = state
    us[32:40, :] = decay
    for dz in (4, 3, 5, 2, 6, 1, 7):
        remote(us, zr.at[z], s_sem.at[3], c_sem.at[2], {"sp_0": (z + dz) % NZ}).start()
    zr[z] = us[...]
    inside(0)
    inside(1)
    take(zr.at[pl.ds(0, NZ - 1)], c_sem.at[2])
    state = jnp.zeros((32, 128), f32)
    for k in range(NZ):
        counts = (k < z).astype(f32)
        state = (1.0 - counts) * state + counts * (zr[k, 32:33, :] * state + zr[k, 0:32, :])
    for k in range(NX):
        isend[k] = px[k, 32:33, :] * state + px[k, 0:32, :]
    for dx in range(NX):
        to = (x + dx) % NX
        for dc in range(NC):
            if dx or dc:
                remote(
                    isend.at[to], inc.at[c * NX + x], s_sem.at[4], c_sem.at[3],
                    {"sp_1": to, "sp_2": (c + dc) % NC},
                ).start()
    inc[c * NX + x] = isend[x]
    take(inc.at[pl.ds(0, NX * NC - 1)], c_sem.at[3])

    loads[4].wait()
    for h in range(2):
        lanes = slice(128 * h, 128 * (h + 1))
        before = inc[NX * h : NX * (h + 1)].reshape(128, 128)
        before = (1.0 - cf) * before + cf * (
            st_recv[h, 128:129, :] * before + st_recv[h, 0:128, :]
        )
        recur = rec[h] + product_nt(qend[:, lanes], before)
        scale = lax.rsqrt(jnp.mean(recur * recur, axis=-1, keepdims=True) + EPS)
        gate_in = ob[:, lanes].astype(f32)
        gated = recur * scale * hg_ref[...] * (gate_in * jax.nn.sigmoid(gate_in))
        gall[p, :, lanes] = gated.astype(bf16)

    for half in range(2):
        rows = pl.ds(128 * half, 128)
        other = pl.ds(128 * (1 - half), 128)
        remote(gall.at[p, rows], gall.at[p, rows], s_sem.at[5], gm.at[half], at_up).start()
        remote(gall.at[p, other], gall.at[p, other], s_sem.at[5], gp.at[1 - half], at_down).start()
    low, high = pl.ds(0, 128), pl.ds(128, 128)
    loads[5].wait()

    def project(source, fresh):
        lhs = gall[source]
        for k in range(4):
            cols = slice(512 * k, 512 * (k + 1))
            part = dot(lhs, wh[source, :, cols])
            if fresh:
                acc[:, cols] = part
            else:
                acc[:, cols] = acc[:, cols] + part

    project(p, True)
    take(gall.at[down, low], gm.at[0])
    remote(gall.at[down, low], gall.at[down, low], s_sem.at[5], gr.at[0], at_up).start()
    take(gall.at[up, high], gp.at[1])
    remote(gall.at[up, high], gall.at[up, high], s_sem.at[5], gr.at[1], at_down).start()
    take(gall.at[down, high], gm.at[1])
    project(down, False)
    take(gall.at[up, low], gp.at[0])
    project(up, False)
    take(wd.at[down, low], wm.at[0])
    remote(wd.at[down, low], wd.at[down, low], s_sem.at[1], wr.at[0], at_up).start()
    take(wd.at[up, high], wp.at[1])
    remote(wd.at[up, high], wd.at[up, high], s_sem.at[1], wr.at[1], at_down).start()
    take(gall.at[far, low], gr.at[0])
    take(gall.at[far, high], gr.at[1])
    project(far, False)

    loads[6].wait()
    gain = fg_ref[...]

    def norm_rows(k, _):
        rows = pl.ds(pl.multiple_of(k * 32, 32), 32)
        wide = (stream[rows, :].astype(f32) + acc[rows, :]).astype(bf16)
        mixed[rows, :] = wide
        wide = wide.astype(f32)
        scale = lax.rsqrt(jnp.mean(wide * wide, axis=-1, keepdims=True) + EPS)
        done = (wide * scale * gain).astype(bf16)
        for quarter in range(4):
            normed[quarter, rows, :] = done[:, 512 * quarter : 512 * (quarter + 1)]
        return 0

    lax.fori_loop(0, ROWS // 32, norm_rows, 0)

    dest0, dest1 = dest_ref[0:1, :], dest_ref[1:2, :]
    slot = lax.broadcasted_iota(jnp.int32, (128, ROWS), 0)

    def dispatch(n, _):
        ids = slot + n * 128
        pick = jnp.where((ids == dest0) | (ids == dest1), 1.0, 0.0).astype(bf16)
        rows = dot(pick, normed[p]).astype(bf16).reshape(8, 16, 512)
        sbuf[pl.ds(n * 8, 8)] = rows
        dz = ring_step(n)
        for j in range(8):
            device = {
                "sp_0": (z + dz) % NZ, "sp_1": (x + j // 2) % NX, "sp_2": (c + j % 2) % NC,
            }

            def send(j=j, device=device):
                remote(
                    sbuf.at[n * 8 + j], xbuf.at[p, n * 8 + j], s_sem.at[6], xs.at[n], device
                ).start()

            if j:
                send()
            else:
                pl.when(n > 0)(send)

                @pl.when(n == 0)
                def _():
                    xbuf[p, 0] = rows[0]

        return 0

    lax.fori_loop(0, NZ, dispatch, 0)
    loads[7].wait()
    loads[8].wait()

    i0 = lax.broadcasted_iota(jnp.int32, (128, 128), 0)
    i1 = lax.broadcasted_iota(jnp.int32, (128, 128), 1)
    gather = ones_where(i1 == ((i0 >> 2) & 7) * 16 + (i0 >> 5) * 4 + (i0 & 3))
    spread = ones_where(i0 == ((i1 >> 2) & 7) * 16 + (i1 >> 5) * 4 + (i1 & 3))

    def stage_forward(n):
        group = pl.ds(n * 8, 8)

        @pl.when(n == 0)
        def _():
            take(xbuf.at[p, pl.ds(1, 7)], xs.at[n])

        @pl.when(n > 0)
        def _():
            take(xbuf.at[p, group], xs.at[n])

        remote(xbuf.at[p, group], xbuf.at[p, group], s_sem.at[7], yfm.at[n], at_up).start()
        remote(xbuf.at[p, group], xbuf.at[p, group], s_sem.at[7], yfp.at[n], at_down).start()

    def stage_relay(n):
        group = pl.ds(n * 8, 8)
        front, back = pl.ds(n * 8, 4), pl.ds(n * 8 + 4, 4)
        take(xbuf.at[down, group], yfm.at[n])
        remote(xbuf.at[down, front], xbuf.at[down, front], s_sem.at[7], yrm.at[n], at_up).start()
        take(xbuf.at[up, group], yfp.at[n])
        remote(xbuf.at[up, back], xbuf.at[up, back], s_sem.at[7], yrp.at[n], at_down).start()

    def stage_hidden(n):
        group = pl.ds(n * 8, 8)
        take(xbuf.at[far, pl.ds(n * 8, 4)], yrm.at[n])
        take(xbuf.at[far, pl.ds(n * 8 + 4, 4)], yrp.at[n])
        rows = jnp.concatenate([xbuf[k, group].reshape(128, 512) for k in range(NY)], axis=1)
        gate = dot(rows, wg[...])
        hidden = (gate * jax.nn.sigmoid(gate) * dot(rows, wu[...])).astype(bf16)
        hidden = dot(gather, hidden).astype(bf16).reshape(NY, 32, 256)
        hsend[n] = hidden
        for dy in range(1, NY):
            to = (p + dy) % NY
            remote(hsend.at[n, to], hrec.at[n, p], s_sem.at[8], hs.at[n], {"tp": to}).start()
        hrec[n, p] = hsend[n, p]

    def stage_down(n):
        take(hrec.at[n, pl.ds(0, NY - 1)], hs.at[n])
        rows = jnp.concatenate([hrec[n, k] for k in range(NY)], axis=1)
        outs = [
            dot(rows, wd[:, :, 512 * k : 512 * (k + 1)].reshape(1024, 512)).astype(bf16)
            for k in range(4)
        ]
        outs = dot(spread, jnp.concatenate(outs, axis=0)).astype(bf16).reshape(8, 16, 512)
        rsend[pl.ds(n * 8, 8)] = outs
        dz = ring_step(n)
        for j in range(8):
            device = {
                "sp_0": (z + NZ - dz) % NZ,
                "sp_1": (x + NX - j // 2) % NX,
                "sp_2": (c + j % 2) % NC,
            }

            def send(j=j, device=device):
                remote(
                    rsend.at[n * 8 + j], rbuf.at[n * 8 + j], s_sem.at[9], rs.at[n], device
                ).start()

            if j:
                send()
            else:
                pl.when(n > 0)(send)

                @pl.when(n == 0)
                def _():
                    rbuf[0] = outs[0]

    def pipeline(i, _):
        @pl.when(i < NZ)
        def _():
            stage_forward(i)

        @pl.when((i >= 1) & (i < NZ + 1))
        def _():
            stage_relay(i - 1)

        @pl.when((i >= 2) & (i < NZ + 2))
        def _():
            stage_hidden(i - 2)

        @pl.when(i == 3)
        def _():
            take(wd.at[down, high], wm.at[1])
            take(wd.at[up, low], wp.at[0])
            take(wd.at[far, low], wr.at[0])
            take(wd.at[far, high], wr.at[1])

        @pl.when(i >= 3)
        def _():
            stage_down(i - 3)

        return 0

    lax.fori_loop(0, NZ + 3, pipeline, 0)

    picks[...] = jnp.zeros_like(picks)
    base = base_ref[...]

    def combine(n, _):
        @pl.when(n == 0)
        def _():
            take(rbuf.at[pl.ds(1, 7)], rs.at[n])

        @pl.when(n > 0)
        def _():
            take(rbuf.at[pl.ds(n * 8, 8)], rs.at[n])

        rows = rbuf[pl.ds(n * 8, 8)].reshape(128, 512)
        for k in range(4):
            pick = jnp.where(i1 + (n * 128 - 4 * k) == base, 1.0, 0.0).astype(bf16)
            picks[k] = picks[k] + dot(pick, rows)
        return 0

    lax.fori_loop(0, NZ, combine, 0)
    own = mixed[pl.ds(pl.multiple_of(p * GROUP, GROUP), GROUP), :]
    for k in range(4):
        cols = slice(512 * k, 512 * (k + 1))
        routed = wsel_ref[:, 0:1] * picks[k, 0:64, :] + wsel_ref[:, 1:2] * picks[k, 64:128, :]
        out_ref[:, cols] = (own[:, cols].astype(f32) + routed).astype(bf16)

    take(st_send, s_sem.at[0])
    take(wd.at[pl.ds(0, 3)], s_sem.at[1])
    take(tq.at[pl.ds(0, 3)], s_sem.at[2])
    take(zr.at[pl.ds(0, 7)], s_sem.at[3])
    take(inc.at[pl.ds(0, 7)], s_sem.at[4])
    take(gall.at[pl.ds(0, 3)], s_sem.at[5])
    take(sbuf.at[pl.ds(0, 63)], s_sem.at[6])
    take(xbuf.at[pl.ds(0, 3)], s_sem.at[7])
    take(hrec.at[pl.ds(0, 6)], s_sem.at[8])
    take(rbuf.at[pl.ds(0, 63)], s_sem.at[9])


def per_device(
    stream, query, forget_gate_logits, value_input_rows, output_gate_logits, forget_floor_margin,
    additional_fading_speed, head_norm_gain, output_head_weight, feedforward_norm_gain,
    selected_expert_index, selected_expert_weight, expert_gate_weight, expert_up_weight,
    expert_down_weight,
):
    z, x, c, p = [lax.axis_index(name) for name in SP_TP]
    blocks = selected_expert_index.reshape(NY, GROUP * 2)
    same = blocks[:, :, None] == blocks[:, None, :]
    earlier = jnp.tril(jnp.ones((GROUP * 2, GROUP * 2), bool), -1)
    rank = jnp.sum((same & earlier).astype(jnp.int32), axis=2)
    dz = (blocks // 8 + NZ - z) % NZ
    group = jnp.where(dz <= 4, jnp.maximum(2 * dz - 1, 0), 2 * (NZ - dz))
    j = ((blocks // 2 % NX + NX - x) % NX) * 2 + (blocks % 2 + c) % NC
    start = (group * 8 + j) * 16 + rank
    dest = start + CAP * jnp.arange(NY, dtype=jnp.int32)[:, None]
    dest = dest.reshape(ROWS, 2).T
    base = lax.dynamic_index_in_dim(start, p, 0, keepdims=False).reshape(GROUP, 2)
    base = base.T.reshape(2 * GROUP, 1)

    vmem = pl.BlockSpec(memory_space=pltpu.VMEM)
    hbm = pl.BlockSpec(memory_space=pl.ANY)
    dma = pltpu.SemaphoreType.DMA
    V = pltpu.VMEM
    return pl.pallas_call(
        kernel,
        name="layer",
        out_shape=jax.ShapeDtypeStruct((GROUP, 2048), bf16),
        in_specs=[vmem] * 7 + [hbm] * 9,
        out_specs=vmem,
        scratch_shapes=[
            V((ROWS, 256), bf16), V((ROWS, 256), bf16), V((ROWS, 256), bf16), V((ROWS, 256), bf16),
            V((ROWS, 2048), bf16), V((4, 256, 2048), bf16), V((2048, 256), bf16),
            V((2048, 256), bf16), V((4, 256, 2048), bf16),
            V((2, ROWS, 128), f32), V((ROWS, 256), f32), V((2, 136, 128), f32),
            V((2, 136, 128), f32), V((4, 40, 128), f32), V((4, 40, 128), f32), V((4, 40, 128), f32),
            V((40, 128), f32), V((8, 40, 128), f32), V((4, 32, 128), f32), V((8, 32, 128), f32),
            V((4, ROWS, 256), bf16), V((ROWS, 2048), f32), V((ROWS, 2048), bf16),
            V((4, ROWS, 512), bf16), V((64, 16, 512), bf16), V((4, 64, 16, 512), bf16),
            V((8, 4, 32, 256), bf16), V((8, 4, 32, 256), bf16), V((64, 16, 512), bf16),
            V((64, 16, 512), bf16), V((4, 128, 512), f32),
            dma((9,)), dma((10,)), dma((4,)), dma((2,)), dma((2,)), dma((2,)), dma((2,)), dma((2,)),
            dma((2,)), dma((8,)), dma((8,)), dma((8,)), dma((8,)), dma((8,)), dma((8,)), dma((8,)),
        ],
        compiler_params=pltpu.CompilerParams(
            collective_id=0, has_side_effects=True, vmem_limit_bytes=60 * 1024 * 1024
        ),
    )(
        dest, base, selected_expert_weight, forget_floor_margin.reshape(1, 256),
        additional_fading_speed, head_norm_gain.reshape(1, 128),
        feedforward_norm_gain.reshape(1, 2048), query, forget_gate_logits, value_input_rows,
        output_gate_logits, stream, output_head_weight.reshape(4, 256, 2048), expert_gate_weight[0],
        expert_up_weight[0], expert_down_weight[0],
    )


def solution(mesh):
    finer = Mesh(mesh.devices.reshape(NZ, NX, NC, mesh.shape["tp"]), SP_TP)
    in_specs = (
        P(SP, None), P(SP, "tp"), P(SP, "tp"), P(SP, "tp"), P(SP, "tp"), P("tp", None),
        P(SP, "tp"), P(), P(), P(), P(SP, None), P(SP_TP, None), P(SP, None, "tp"),
        P(SP, None, "tp"), P(SP, "tp", None),
    )
    return jax.shard_map(
        per_device, mesh=finer, in_specs=in_specs, out_specs=P(SP_TP, None), check_vma=False
    )
```

time: 355 us -> 125 us (0.35)
  waiting for transfers between devices: 170 us -> 0 us
  Pallas kernels: 0 us -> 117 us
  blocking collectives: 94 us -> 0 us
  local copies, waits for them, and re-layouts: 28.3 us -> 6.84 us
  other arithmetic: 19.7 us -> 1.66 us
  matrix products: 17.7 us -> 0 us
  between operations: 13.5 us -> 0.05 us
  starting transfers between devices: 10.8 us -> 0 us
    pallas_call x0 -> x1, Pallas kernels: none -> 117 us  [per_device(): pl.pallas_call(kernel, name='layer', out_shape=jax.ShapeDtypeStruct((GROU...]
    reduce_scatter x1 -> x0, waiting for transfers between devices: 83.7 us -> none  [per_device(): lax.psum_scatter(jnp.dot(hidden_flat, w_down, preferred_element_type=f32)...]
    all_gather x2 -> x0, waiting for transfers between devices: 59.6 us -> none  [the longest x1 47 us: on_gathered_pieces(): blocks = [lax.all_gather(share, axis) for share in pieces]]
    all_gather x6 -> x0, blocking collectives: 50.3 us -> none  [the longest x5 40 us: carried_in(): pieces = jax.tree.map(lambda part: lax.all_gather(part, axis), subtotal)]
    all_to_all x1 -> x0, blocking collectives: 43.7 us -> none  [per_device(): lax.all_to_all(outgoing, SP, split_axis=1, concat_axis=1, tiled=True)]
    all_to_all x1 -> x0, waiting for transfers between devices: 26.5 us -> none  [per_device(): lax.all_to_all(expert_out, SP, split_axis=0, concat_axis=0, tiled=True)]
    dot_general x8 -> x0, matrix products: 17.7 us -> none  [the longest x1 4.48 us: per_device(): jnp.dot(hidden_flat, w_down, preferred_element_type=f32)]
    reshape x6 -> x2, local copies, waits for them, and re-layouts: 11.6 us -> 0.91 us  [the longest x1 0.78 us: per_device(): base = base.T.reshape(2 * GROUP, 1)]
  transfers between devices with their start and end apart: 4 -> 0, of which waited for: 4 -> 0; matrix products, arithmetic and copies ran while one was open for 3% -> 0% of each run, Pallas kernels for 0% -> 0%
where the time goes in v1:
time: 125 us
  Pallas kernels  117 us (94%)
  local copies, waits for them, and re-layouts  6.84 us (5%)
  other arithmetic  1.66 us (1%)
    pallas_call x1, Pallas kernels, per_device(): pl.pallas_call(kernel, name='layer', out_shape=jax.ShapeDtypeStruct((GROU...  117 us
    unnamed x4, local copies, waits for them, and re-layouts  5.33 us

profile of v1, /device:TPU:1, one launch (start us, length us, event | category | flops | bytes accessed | tf_op | source)
XLA Modules:
  0.0 125.2 jit_solution(8590590011417426757)
XLA Ops:
  0.0 0.1 add.124
  0.1 0.1 add.125
  0.2 0.1 iota_compare_fusion
  0.3 1.4 %copy.30.wsel_ref = f32[64,2]{1,0:T(8,128)} copy(f32[64,2]{0,1:T(2,128)} %param.26) | data formatting | bytes 1024 | tf_op args[11]
  1.6 1.5 %copy.31.fade_ref = f32[256,2]{1,0:T(8,128)} copy(f32[256,2]{0,1:T(2,128)} %param.21) | data formatting | bytes 4096 | tf_op args[6]
  3.1 0.8 copy.26
  3.9 0.1 eq.21
  4.1 0.2 convert_reduce_fusion
  4.4 0.1 reshape.43
  4.5 0.1 copy.28
  4.6 0.8 reshape.49.base_ref
  5.4 0.1 reduce_sum.12
  5.5 0.1 copy.27
  5.6 1.3 %add_bitcast_fusion.dest_ref = s32[2,256]{1,0:T(2,128)} fusion(s32[256,2]{0,1:T(2,128)S(1)} %copy.27, s32[256,2]{0,1:T(2,128)} %param.25, s32[256]{0:T(256)S(1)} %add.125, s32[]{:T(128)S(6)} %axis_index.49, s32[]{:T(128)S(6)} %axis_index.46, s32[]{:T(128)S(6)} %axis_index.43), kind=kLoop, calls=%fused_computation.70 | loop fusion | flops 47104 | bytes 7180 | tf_op jit(solution)/shard_map/transpose | solution.py:478
  6.9 116.6 %layer.1 = bf16[64,2048]{1,0:T(8,128)(2,1)} custom-call(s32[2,256]{1,0:T(2,128)} %add_bitcast_fusion.dest_ref, s32[128,1]{1,0:T(8,128)} %reshape.49.base_ref, f32[64,2]{1,0:T(8,128)} %copy.30.wsel_ref, f32[1,256]{1,0:T(1,128)} %bitcast.16, f32[256,2]{1,0:T(8,128)} %copy.31.fade_ref, f32[1,128]{1,0:T(1,128)} %bitcast.17, f32[1,2048]{1,0:T(1,128)} %bitcast.15, ...), custom_call_target="tpu_custom_call" | custom-call | tf_op jit(solution)/shard_map/layer/pallas_call | solution.py:486
  123.5 1.7 %copy.33 = bf16[64,2048]{1,0:T(8,128)(2,1)} copy(bf16[64,2048]{1,0:T(8,128)(2,1)} %layer.1) | data formatting | bytes 524288
  (4 shorter events, 0.1 us)

commit v2 on v1

--- a/solution.py
+++ b/solution.py
@@ -46,8 +46,12 @@
     return dot_nt(jnp.concatenate([ah, ah, al], axis=1), jnp.concatenate([bh, bl, bh], axis=1))
 
 
+ORDER = (0, 5, 4, 6, 3, 7, 2, 1)
+PACKED = sum(dz << (3 * n) for n, dz in enumerate(ORDER))
+
+
 def ring_step(n):
-    return (NZ + ((n + 1) // 2) * (1 - 2 * ((n + 1) % 2))) % NZ
+    return (PACKED >> (3 * n)) & 7
 
 
 def remote(src, dst, send_sem, recv_sem, device):
@@ -66,11 +70,11 @@
 
 
 def kernel(
-    dest_ref, base_ref, wsel_ref, mar_ref, fade_ref, hg_ref, fg_ref,
+    idx_ref, wsel_ref, mar_ref, fade_ref, hg_ref, fg_ref,
     q_hbm, f_hbm, v_hbm, og_hbm, stream_hbm, wh_hbm, wg_hbm, wu_hbm, wd_hbm,
     out_ref,
     qb, fb, vb, ob, stream, wh, wg, wu, wd,
-    rec, qend, st_send, st_recv, tq, xr, px, us, zr, isend, inc,
+    rec, qend, cs, cr, px, us, zr, isend, inc, dest, dcol,
     gall, acc, mixed, normed, sbuf, xbuf, hsend, hrec, rsend, rbuf, picks,
     load_sem, s_sem, c_sem, gm, gp, gr, wm, wp, wr, xs, yfm, yfp, yrm, yrp, hs, rs,
 ):
@@ -102,11 +106,14 @@
         )
         return 0
 
-    lax.fori_loop(1, NZ * NX * NC, greet, 0)
     for peer in (up, down, far):
         pl.semaphore_signal(
             barrier, inc=1, device_id={"tp": peer}, device_id_type=pl.DeviceIdType.MESH
         )
+    lax.fori_loop(1, NZ * NX * NC, greet, 0)
+
+    def as_column(line, width):
+        return jnp.transpose(jnp.broadcast_to(line, (width, line.shape[1])), (1, 0))
 
     row = lax.broadcasted_iota(jnp.int32, (ROWS, ROWS), 0)
     col = lax.broadcasted_iota(jnp.int32, (ROWS, ROWS), 1)
@@ -118,47 +125,6 @@
         odd = ((row >> shift) & 1) == 1
         same = (row >> shift) == (col >> shift)
         return ones_where(same & ((odd & (col <= row)) | (jnp.logical_not(odd) & (col > row))))
-
-    loads[0].wait()
-    margin = mar_ref[...]
-    keys = margin * jax.nn.sigmoid(-fb[...].astype(f32))
-    fade = fade_ref[...]
-    fades = jnp.concatenate(
-        [jnp.broadcast_to(fade[:, h : h + 1], (ROWS, 128)) for h in range(2)], axis=1
-    )
-    log_decay = jnp.log1p(-keys) + fades
-    parts = jnp.concatenate(split3(log_decay), axis=1)
-
-    def sums(matrix):
-        three = dot(matrix, parts)
-        return three[:, 0:256] + (three[:, 256:512] + three[:, 512:768])
-
-    loads[1].wait()
-    loads[2].wait()
-    queries = qb[...].astype(f32)
-    to_start = sums(ones_where(col <= row))
-    to_end = sums(ones_where(col > row))
-    qend[...] = queries * jnp.exp(to_start)
-    kend = keys * jnp.exp(to_end)
-    total = jnp.exp(to_start[ROWS - 1 : ROWS, :])
-    vt = jnp.transpose(vb[...].astype(f32), (1, 0)).astype(bf16)
-    for h in range(2):
-        lanes = slice(128 * h, 128 * (h + 1))
-        kh, kl = split2(kend[:, lanes])
-        both = dot(vt[lanes, :], jnp.concatenate([kh, kl], axis=1))
-        st_send[h, 0:128, :] = both[:, 0:128] + both[:, 128:256]
-        st_send[h, 128:136, :] = jnp.broadcast_to(total[:, lanes], (8, 128))
-
-    pl.semaphore_wait(barrier, NZ * NX * NC - 1 + 3)
-
-    to_core = remote(st_send, st_recv, s_sem.at[0], c_sem.at[0], {"sp_2": 1 - c})
-    to_core.start()
-    loads[3].wait()
-    for half in range(2):
-        rows = pl.ds(128 * half, 128)
-        other = pl.ds(128 * (1 - half), 128)
-        remote(wd.at[p, rows], wd.at[p, rows], s_sem.at[1], wm.at[half], at_up).start()
-        remote(wd.at[p, other], wd.at[p, other], s_sem.at[1], wp.at[1 - half], at_down).start()
 
     def inside(h):
         lanes = slice(128 * h, 128 * (h + 1))
@@ -177,60 +143,117 @@
         vh = vb[:, lanes]
         rec[h] = dot(sh, vh) + dot(sl, vh)
 
-    take(st_recv, c_sem.at[0])
-    cf = c.astype(f32)
-    own, other = st_send[c], st_recv[c]
-    first = own * (1.0 - cf) + other * cf
-    second = other * (1.0 - cf) + own * cf
-    chip_state = second[128:129, :] * first[0:128, :] + second[0:128, :]
-    chip_decay = first[128:136, :] * second[128:136, :]
-    for k in range(NX):
-        tq[k, 0:32, :] = chip_state[32 * k : 32 * (k + 1), :]
-        tq[k, 32:40, :] = chip_decay
-    for dx in range(1, NX):
+    loads[0].wait()
+    margin = jnp.concatenate([mar_ref[0:1, :], mar_ref[1:2, :]], axis=1)
+    keys = margin * jax.nn.sigmoid(-fb[...].astype(f32))
+    fades = jnp.concatenate([as_column(fade_ref[h : h + 1, :], 128) for h in range(2)], axis=1)
+    log_decay = jnp.log1p(-keys) + fades
+    parts = jnp.concatenate(split3(log_decay), axis=1)
+
+    def sums(matrix):
+        three = dot(matrix, parts)
+        return three[:, 0:256] + (three[:, 256:512] + three[:, 512:768])
+
+    loads[1].wait()
+    loads[2].wait()
+    queries = qb[...].astype(f32)
+    to_start = sums(ones_where(col <= row))
+    to_end = sums(ones_where(col > row))
+    qend[...] = queries * jnp.exp(to_start)
+    kend = keys * jnp.exp(to_end)
+    total = jnp.exp(to_start[ROWS - 1 : ROWS, :])
+    vt = jnp.transpose(vb[...].astype(f32), (1, 0)).astype(bf16)
+    for h in range(2):
+        lanes = slice(128 * h, 128 * (h + 1))
+        kh, kl = split2(kend[:, lanes])
+        both = dot(vt[lanes, :], jnp.concatenate([kh, kl], axis=1))
+        both = both[:, 0:128] + both[:, 128:256]
+        for k in range(NX):
+            cs[k * NC + h, 0:32, :] = both[32 * k : 32 * (k + 1), :]
+            cs[k * NC + h, 32:40, :] = jnp.broadcast_to(total[:, lanes], (8, 128))
+    sums_of = {shift: sums(level_sum(shift)) for shift in (3, 4, 5, 6, 7)}
+    inside(0)
+    inside(1)
+
+    chosen = [idx_ref[k : k + 1, :].astype(f32) for k in range(2)]
+    columns = [as_column(e, ROWS) for e in chosen]
+    block = (row >> 6) == (col >> 6)
+    before = block & (row < col)
+
+    def count(condition):
+        return jnp.sum(jnp.where(condition, 1.0, 0.0), axis=0, keepdims=True)
+
+    ranks = [
+        count(before & (columns[0] == chosen[0])),
+        count(block & (columns[0] == chosen[1])) + count(before & (columns[1] == chosen[1])),
+    ]
+    first_slot = CAP * (lax.broadcasted_iota(jnp.int32, (1, ROWS), 1) >> 6)
+    for k in range(2):
+        expert = idx_ref[k : k + 1, :]
+        dz = ((expert >> 3) + NZ - z) & 7
+        group = jnp.zeros_like(dz)
+        for n, offset in enumerate(ORDER):
+            group = jnp.where(dz == offset, n, group)
+        j = (((expert >> 1) + NX - x) & 3) * 2 + ((expert + c) & 1)
+        place = ((group * 8 + j) * 16 + first_slot).astype(f32) + ranks[k]
+        dest[k : k + 1, :] = place
+        dcol[k] = as_column(place, 128)
+
+    pl.semaphore_wait(barrier, NZ * NX * NC - 1 + 3)
+
+    def down_weights(n):
+        rows, other = pl.ds(64 * n, 64), pl.ds(64 * (3 - n), 64)
+        remote(wd.at[p, rows], wd.at[p, rows], s_sem.at[1], wm.at[n], at_up).start()
+        remote(wd.at[p, other], wd.at[p, other], s_sem.at[1], wp.at[3 - n], at_down).start()
+
+    for dx in (2, 1, 3, 0):
         to = (x + dx) % NX
-        remote(tq.at[to], xr.at[x], s_sem.at[2], c_sem.at[1], {"sp_1": to}).start()
-    xr[x] = tq[x]
-    sums_of = {shift: sums(level_sum(shift)) for shift in (3, 4, 5, 6, 7)}
-    take(xr.at[pl.ds(0, NX - 1)], c_sem.at[1])
+        for dc in range(NC):
+            if dx or dc:
+                head = (c + dc) % NC
+                remote(
+                    cs.at[to * NC + head], cr.at[x * NC + c], s_sem.at[2], c_sem.at[1],
+                    {"sp_1": to, "sp_2": head},
+                ).start()
+    loads[3].wait()
+    down_weights(0)
+    down_weights(1)
+    cr[x * NC + c] = cs[x * NC + c]
+    take(cr.at[pl.ds(0, NX * NC - 1)], c_sem.at[1])
     state, decay = jnp.zeros((32, 128), f32), jnp.ones((8, 128), f32)
-    for k in range(NX):
+    for k in range(NX * NC):
         px[k, 0:32, :] = state
         px[k, 32:40, :] = decay
-        state = xr[k, 32:33, :] * state + xr[k, 0:32, :]
-        decay = xr[k, 32:40, :] * decay
+        state = cr[k, 32:33, :] * state + cr[k, 0:32, :]
+        decay = cr[k, 32:40, :] * decay
     us[0:32, :] = state
     us[32:40, :] = decay
     for dz in (4, 3, 5, 2, 6, 1, 7):
         remote(us, zr.at[z], s_sem.at[3], c_sem.at[2], {"sp_0": (z + dz) % NZ}).start()
     zr[z] = us[...]
-    inside(0)
-    inside(1)
     take(zr.at[pl.ds(0, NZ - 1)], c_sem.at[2])
     state = jnp.zeros((32, 128), f32)
     for k in range(NZ):
         counts = (k < z).astype(f32)
         state = (1.0 - counts) * state + counts * (zr[k, 32:33, :] * state + zr[k, 0:32, :])
-    for k in range(NX):
+    for k in range(NX * NC):
         isend[k] = px[k, 32:33, :] * state + px[k, 0:32, :]
-    for dx in range(NX):
+    for dx in (2, 1, 3, 0):
         to = (x + dx) % NX
         for dc in range(NC):
             if dx or dc:
+                core = (c + dc) % NC
                 remote(
-                    isend.at[to], inc.at[c * NX + x], s_sem.at[4], c_sem.at[3],
-                    {"sp_1": to, "sp_2": (c + dc) % NC},
+                    isend.at[to * NC + core], inc.at[c * NX + x], s_sem.at[4], c_sem.at[3],
+                    {"sp_1": to, "sp_2": core},
                 ).start()
-    inc[c * NX + x] = isend[x]
+    inc[c * NX + x] = isend[x * NC + c]
     take(inc.at[pl.ds(0, NX * NC - 1)], c_sem.at[3])
 
     loads[4].wait()
     for h in range(2):
         lanes = slice(128 * h, 128 * (h + 1))
         before = inc[NX * h : NX * (h + 1)].reshape(128, 128)
-        before = (1.0 - cf) * before + cf * (
-            st_recv[h, 128:129, :] * before + st_recv[h, 0:128, :]
-        )
         recur = rec[h] + product_nt(qend[:, lanes], before)
         scale = lax.rsqrt(jnp.mean(recur * recur, axis=-1, keepdims=True) + EPS)
         gate_in = ob[:, lanes].astype(f32)
@@ -260,14 +283,18 @@
     remote(gall.at[down, low], gall.at[down, low], s_sem.at[5], gr.at[0], at_up).start()
     take(gall.at[up, high], gp.at[1])
     remote(gall.at[up, high], gall.at[up, high], s_sem.at[5], gr.at[1], at_down).start()
+    down_weights(2)
+    for n in range(2):
+        rows, other = pl.ds(64 * n, 64), pl.ds(64 * (3 - n), 64)
+        take(wd.at[down, rows], wm.at[n])
+        remote(wd.at[down, rows], wd.at[down, rows], s_sem.at[1], wr.at[n], at_up).start()
+        take(wd.at[up, other], wp.at[3 - n])
+        remote(wd.at[up, other], wd.at[up, other], s_sem.at[1], wr.at[3 - n], at_down).start()
+    down_weights(3)
     take(gall.at[down, high], gm.at[1])
     project(down, False)
     take(gall.at[up, low], gp.at[0])
     project(up, False)
-    take(wd.at[down, low], wm.at[0])
-    remote(wd.at[down, low], wd.at[down, low], s_sem.at[1], wr.at[0], at_up).start()
-    take(wd.at[up, high], wp.at[1])
-    remote(wd.at[up, high], wd.at[up, high], s_sem.at[1], wr.at[1], at_down).start()
     take(gall.at[far, low], gr.at[0])
     take(gall.at[far, high], gr.at[1])
     project(far, False)
@@ -288,11 +315,11 @@
 
     lax.fori_loop(0, ROWS // 32, norm_rows, 0)
 
-    dest0, dest1 = dest_ref[0:1, :], dest_ref[1:2, :]
+    dest0, dest1 = dest[0:1, :], dest[1:2, :]
     slot = lax.broadcasted_iota(jnp.int32, (128, ROWS), 0)
 
     def dispatch(n, _):
-        ids = slot + n * 128
+        ids = (slot + n * 128).astype(f32)
         pick = jnp.where((ids == dest0) | (ids == dest1), 1.0, 0.0).astype(bf16)
         rows = dot(pick, normed[p]).astype(bf16).reshape(8, 16, 512)
         sbuf[pl.ds(n * 8, 8)] = rows
@@ -316,6 +343,7 @@
                 def _():
                     xbuf[p, 0] = rows[0]
 
+
         return 0
 
     lax.fori_loop(0, NZ, dispatch, 0)
@@ -343,7 +371,7 @@
 
     def stage_relay(n):
         group = pl.ds(n * 8, 8)
-        front, back = pl.ds(n * 8, 4), pl.ds(n * 8 + 4, 4)
+        front, back = pl.ds(n * 8, 3), pl.ds(n * 8 + 3, 5)
         take(xbuf.at[down, group], yfm.at[n])
         remote(xbuf.at[down, front], xbuf.at[down, front], s_sem.at[7], yrm.at[n], at_up).start()
         take(xbuf.at[up, group], yfp.at[n])
@@ -351,8 +379,8 @@
 
     def stage_hidden(n):
         group = pl.ds(n * 8, 8)
-        take(xbuf.at[far, pl.ds(n * 8, 4)], yrm.at[n])
-        take(xbuf.at[far, pl.ds(n * 8 + 4, 4)], yrp.at[n])
+        take(xbuf.at[far, pl.ds(n * 8, 3)], yrm.at[n])
+        take(xbuf.at[far, pl.ds(n * 8 + 3, 5)], yrp.at[n])
         rows = jnp.concatenate([xbuf[k, group].reshape(128, 512) for k in range(NY)], axis=1)
         gate = dot(rows, wg[...])
         hidden = (gate * jax.nn.sigmoid(gate) * dot(rows, wu[...])).astype(bf16)
@@ -394,6 +422,7 @@
                 def _():
                     rbuf[0] = outs[0]
 
+
     def pipeline(i, _):
         @pl.when(i < NZ)
         def _():
@@ -409,10 +438,11 @@
 
         @pl.when(i == 3)
         def _():
-            take(wd.at[down, high], wm.at[1])
-            take(wd.at[up, low], wp.at[0])
-            take(wd.at[far, low], wr.at[0])
-            take(wd.at[far, high], wr.at[1])
+            for n in range(2):
+                take(wd.at[down, pl.ds(64 * (n + 2), 64)], wm.at[n + 2])
+                take(wd.at[up, pl.ds(64 * n, 64)], wp.at[n])
+            for n in range(4):
+                take(wd.at[far, pl.ds(64 * n, 64)], wr.at[n])
 
         @pl.when(i >= 3)
         def _():
@@ -423,7 +453,9 @@
     lax.fori_loop(0, NZ + 3, pipeline, 0)
 
     picks[...] = jnp.zeros_like(picks)
-    base = base_ref[...]
+    own_rows = pl.ds(pl.multiple_of(p * GROUP, GROUP), GROUP)
+    base = jnp.concatenate([dcol[0, own_rows, :], dcol[1, own_rows, :]], axis=0)
+    base = base - (CAP * p).astype(f32)
 
     def combine(n, _):
         @pl.when(n == 0)
@@ -436,20 +468,21 @@
 
         rows = rbuf[pl.ds(n * 8, 8)].reshape(128, 512)
         for k in range(4):
-            pick = jnp.where(i1 + (n * 128 - 4 * k) == base, 1.0, 0.0).astype(bf16)
+            pick = jnp.where((i1 + (n * 128 - 4 * k)).astype(f32) == base, 1.0, 0.0).astype(bf16)
             picks[k] = picks[k] + dot(pick, rows)
         return 0
 
     lax.fori_loop(0, NZ, combine, 0)
-    own = mixed[pl.ds(pl.multiple_of(p * GROUP, GROUP), GROUP), :]
+    own = mixed[own_rows, :]
+    weight = as_column(jnp.concatenate([wsel_ref[0:1, :], wsel_ref[1:2, :]], axis=1), 128)
     for k in range(4):
         cols = slice(512 * k, 512 * (k + 1))
-        routed = wsel_ref[:, 0:1] * picks[k, 0:64, :] + wsel_ref[:, 1:2] * picks[k, 64:128, :]
+        weighted = weight[:, 0:1] * picks[k]
+        routed = weighted[0:64, :] + weighted[64:128, :]
         out_ref[:, cols] = (own[:, cols].astype(f32) + routed).astype(bf16)
 
-    take(st_send, s_sem.at[0])
     take(wd.at[pl.ds(0, 3)], s_sem.at[1])
-    take(tq.at[pl.ds(0, 3)], s_sem.at[2])
+    take(cr.at[pl.ds(0, 7)], s_sem.at[2])
     take(zr.at[pl.ds(0, 7)], s_sem.at[3])
     take(inc.at[pl.ds(0, 7)], s_sem.at[4])
     take(gall.at[pl.ds(0, 3)], s_sem.at[5])
@@ -465,20 +498,6 @@
     selected_expert_index, selected_expert_weight, expert_gate_weight, expert_up_weight,
     expert_down_weight,
 ):
-    z, x, c, p = [lax.axis_index(name) for name in SP_TP]
-    blocks = selected_expert_index.reshape(NY, GROUP * 2)
-    same = blocks[:, :, None] == blocks[:, None, :]
-    earlier = jnp.tril(jnp.ones((GROUP * 2, GROUP * 2), bool), -1)
-    rank = jnp.sum((same & earlier).astype(jnp.int32), axis=2)
-    dz = (blocks // 8 + NZ - z) % NZ
-    group = jnp.where(dz <= 4, jnp.maximum(2 * dz - 1, 0), 2 * (NZ - dz))
-    j = ((blocks // 2 % NX + NX - x) % NX) * 2 + (blocks % 2 + c) % NC
-    start = (group * 8 + j) * 16 + rank
-    dest = start + CAP * jnp.arange(NY, dtype=jnp.int32)[:, None]
-    dest = dest.reshape(ROWS, 2).T
-    base = lax.dynamic_index_in_dim(start, p, 0, keepdims=False).reshape(GROUP, 2)
-    base = base.T.reshape(2 * GROUP, 1)
-
     vmem = pl.BlockSpec(memory_space=pltpu.VMEM)
     hbm = pl.BlockSpec(memory_space=pl.ANY)
     dma = pltpu.SemaphoreType.DMA
@@ -487,28 +506,28 @@
         kernel,
         name="layer",
         out_shape=jax.ShapeDtypeStruct((GROUP, 2048), bf16),
-        in_specs=[vmem] * 7 + [hbm] * 9,
+        in_specs=[vmem] * 6 + [hbm] * 9,
         out_specs=vmem,
         scratch_shapes=[
             V((ROWS, 256), bf16), V((ROWS, 256), bf16), V((ROWS, 256), bf16), V((ROWS, 256), bf16),
             V((ROWS, 2048), bf16), V((4, 256, 2048), bf16), V((2048, 256), bf16),
             V((2048, 256), bf16), V((4, 256, 2048), bf16),
-            V((2, ROWS, 128), f32), V((ROWS, 256), f32), V((2, 136, 128), f32),
-            V((2, 136, 128), f32), V((4, 40, 128), f32), V((4, 40, 128), f32), V((4, 40, 128), f32),
-            V((40, 128), f32), V((8, 40, 128), f32), V((4, 32, 128), f32), V((8, 32, 128), f32),
+            V((2, ROWS, 128), f32), V((ROWS, 256), f32), V((8, 40, 128), f32), V((8, 40, 128), f32),
+            V((8, 40, 128), f32), V((40, 128), f32), V((8, 40, 128), f32), V((8, 32, 128), f32),
+            V((8, 32, 128), f32), V((2, ROWS), f32), V((2, ROWS, 128), f32),
             V((4, ROWS, 256), bf16), V((ROWS, 2048), f32), V((ROWS, 2048), bf16),
             V((4, ROWS, 512), bf16), V((64, 16, 512), bf16), V((4, 64, 16, 512), bf16),
             V((8, 4, 32, 256), bf16), V((8, 4, 32, 256), bf16), V((64, 16, 512), bf16),
             V((64, 16, 512), bf16), V((4, 128, 512), f32),
-            dma((9,)), dma((10,)), dma((4,)), dma((2,)), dma((2,)), dma((2,)), dma((2,)), dma((2,)),
-            dma((2,)), dma((8,)), dma((8,)), dma((8,)), dma((8,)), dma((8,)), dma((8,)), dma((8,)),
+            dma((9,)), dma((10,)), dma((4,)), dma((2,)), dma((2,)), dma((2,)), dma((4,)), dma((4,)),
+            dma((4,)), dma((8,)), dma((8,)), dma((8,)), dma((8,)), dma((8,)), dma((8,)), dma((8,)),
         ],
         compiler_params=pltpu.CompilerParams(
             collective_id=0, has_side_effects=True, vmem_limit_bytes=60 * 1024 * 1024
         ),
     )(
-        dest, base, selected_expert_weight, forget_floor_margin.reshape(1, 256),
-        additional_fading_speed, head_norm_gain.reshape(1, 128),
+        selected_expert_index.T, selected_expert_weight.T, forget_floor_margin,
+        additional_fading_speed.T, head_norm_gain.reshape(1, 128),
         feedforward_norm_gain.reshape(1, 2048), query, forget_gate_logits, value_input_rows,
         output_gate_logits, stream, output_head_weight.reshape(4, 256, 2048), expert_gate_weight[0],
         expert_up_weight[0], expert_down_weight[0],

time: 125 us -> 115 us (0.920)
  local copies, waits for them, and re-layouts: 6.84 us -> 1.67 us
  Pallas kernels: 117 us -> 113 us
  other arithmetic: 1.66 us -> 0 us
    pallas_call x1, Pallas kernels: 117 us -> 113 us  [per_device(): pl.pallas_call(kernel, name='layer', out_shape=jax.ShapeDtypeStruct((GROU...]
    unnamed x4 -> x1, local copies, waits for them, and re-layouts: 5.33 us -> 1.67 us
    transpose x1 -> x0, other arithmetic: 1.29 us -> none  [per_device(): dest = dest.reshape(ROWS, 2).T]
where the time goes in v2:
time: 115 us; the launch traced here: 114 us
  Pallas kernels  113 us (98%)
  local copies, waits for them, and re-layouts  1.67 us (1%)
    pallas_call x1, Pallas kernels, per_device(): pl.pallas_call(kernel, name='layer', out_shape=jax.ShapeDtypeStruct((GROU...  113 us

profile of v2, /device:TPU:1, one launch (start us, length us, event | category | flops | bytes accessed | tf_op | source)
XLA Modules:
  0.0 114.5 jit_solution(2680350257081207468)
XLA Ops:
  0.0 112.8 %layer.1 = bf16[64,2048]{1,0:T(8,128)(2,1)} custom-call(s32[2,256]{1,0:T(2,128)} %bitcast.14, f32[2,64]{1,0:T(2,128)} %bitcast.16, f32[2,128]{1,0:T(2,128)} %mar_ref.1, f32[2,256]{1,0:T(2,128)} %bitcast.15, f32[1,128]{1,0:T(1,128)} %bitcast.17, f32[1,2048]{1,0:T(1,128)} %bitcast.13, bf16[256,256]{1,0:T(8,128)(2,1)} %q_hbm.1, bf16[256,256]{1,0:T(8,128)(2,1)} %f_hbm.1, ...), custom_call_target="tpu_custom_call" | custom-call | tf_op jit(solution)/shard_map/layer/pallas_call | solution.py:505
  112.8 1.7 %copy.17 = bf16[64,2048]{1,0:T(8,128)(2,1)} copy(bf16[64,2048]{1,0:T(8,128)(2,1)} %layer.1) | data formatting | bytes 524288

commit v3 on v2

--- a/solution.py
+++ b/solution.py
@@ -46,7 +46,8 @@
     return dot_nt(jnp.concatenate([ah, ah, al], axis=1), jnp.concatenate([bh, bl, bh], axis=1))
 
 
-ORDER = (0, 5, 4, 6, 3, 7, 2, 1)
+ORDER = (0, 4, 3, 5, 6, 2, 7, 1)
+NEAR = 6
 PACKED = sum(dz << (3 * n) for n, dz in enumerate(ORDER))
 
 
@@ -74,8 +75,8 @@
     q_hbm, f_hbm, v_hbm, og_hbm, stream_hbm, wh_hbm, wg_hbm, wu_hbm, wd_hbm,
     out_ref,
     qb, fb, vb, ob, stream, wh, wg, wu, wd,
-    rec, qend, cs, cr, px, us, zr, isend, inc, dest, dcol,
-    gall, acc, mixed, normed, sbuf, xbuf, hsend, hrec, rsend, rbuf, picks,
+    rec, qend, cs, csd, cr, crd, px, pxd, us, usd, zr, zrd, isend, inc, dest, dcol,
+    gall, acc, mixed, normed, sbuf, xbuf, hsend, hrec, rsend, rbuf, picks, sdir,
     load_sem, s_sem, c_sem, gm, gp, gr, wm, wp, wr, xs, yfm, yfp, yrm, yrp, hs, rs,
 ):
     z, x, c, p = [lax.axis_index(name) for name in SP_TP]
@@ -96,21 +97,26 @@
 
     barrier = pltpu.get_barrier_semaphore()
 
-    def greet(k, _):
-        dz, dx, dc = k // 8, (k // 2) % 4, k % 2
-        pl.semaphore_signal(
-            barrier,
-            inc=1,
-            device_id={"sp_0": (z + dz) % NZ, "sp_1": (x + dx) % NX, "sp_2": (c + dc) % NC},
-            device_id_type=pl.DeviceIdType.MESH,
-        )
-        return 0
+    def greet(dz, first):
+        for k in range(first, NX * NC):
+            pl.semaphore_signal(
+                barrier,
+                inc=1,
+                device_id={
+                    "sp_0": (z + dz) % NZ, "sp_1": (x + k // 2) % NX, "sp_2": (c + k % 2) % NC,
+                },
+                device_id_type=pl.DeviceIdType.MESH,
+            )
 
     for peer in (up, down, far):
         pl.semaphore_signal(
             barrier, inc=1, device_id={"tp": peer}, device_id_type=pl.DeviceIdType.MESH
         )
-    lax.fori_loop(1, NZ * NX * NC, greet, 0)
+    @pl.loop(1, NZ)
+    def _(dz):
+        greet(dz, 0)
+
+    greet(0, 1)
 
     def as_column(line, width):
         return jnp.transpose(jnp.broadcast_to(line, (width, line.shape[1])), (1, 0))
@@ -169,8 +175,8 @@
         both = dot(vt[lanes, :], jnp.concatenate([kh, kl], axis=1))
         both = both[:, 0:128] + both[:, 128:256]
         for k in range(NX):
-            cs[k * NC + h, 0:32, :] = both[32 * k : 32 * (k + 1), :]
-            cs[k * NC + h, 32:40, :] = jnp.broadcast_to(total[:, lanes], (8, 128))
+            cs[k * NC + h] = both[32 * k : 32 * (k + 1), :]
+            csd[k * NC + h] = total[:, lanes]
     sums_of = {shift: sums(level_sum(shift)) for shift in (3, 4, 5, 6, 7)}
     inside(0)
     inside(1)
@@ -202,42 +208,51 @@
     pl.semaphore_wait(barrier, NZ * NX * NC - 1 + 3)
 
     def down_weights(n):
-        rows, other = pl.ds(64 * n, 64), pl.ds(64 * (3 - n), 64)
+        rows, other = pl.ds(32 * n, 32), pl.ds(32 * (7 - n), 32)
         remote(wd.at[p, rows], wd.at[p, rows], s_sem.at[1], wm.at[n], at_up).start()
-        remote(wd.at[p, other], wd.at[p, other], s_sem.at[1], wp.at[3 - n], at_down).start()
+        remote(wd.at[p, other], wd.at[p, other], s_sem.at[1], wp.at[7 - n], at_down).start()
 
     for dx in (2, 1, 3, 0):
         to = (x + dx) % NX
         for dc in range(NC):
             if dx or dc:
                 head = (c + dc) % NC
+                device = {"sp_1": to, "sp_2": head}
                 remote(
-                    cs.at[to * NC + head], cr.at[x * NC + c], s_sem.at[2], c_sem.at[1],
-                    {"sp_1": to, "sp_2": head},
+                    cs.at[to * NC + head], cr.at[x * NC + c], s_sem.at[2], c_sem.at[1], device
+                ).start()
+                remote(
+                    csd.at[to * NC + head], crd.at[x * NC + c], s_sem.at[10], c_sem.at[0], device
                 ).start()
     loads[3].wait()
-    down_weights(0)
-    down_weights(1)
+    for n in range(4):
+        down_weights(n)
     cr[x * NC + c] = cs[x * NC + c]
+    crd[x * NC + c] = csd[x * NC + c]
     take(cr.at[pl.ds(0, NX * NC - 1)], c_sem.at[1])
-    state, decay = jnp.zeros((32, 128), f32), jnp.ones((8, 128), f32)
+    take(crd.at[pl.ds(0, NX * NC - 1)], c_sem.at[0])
+    state, decay = jnp.zeros((32, 128), f32), jnp.ones((1, 128), f32)
     for k in range(NX * NC):
-        px[k, 0:32, :] = state
-        px[k, 32:40, :] = decay
-        state = cr[k, 32:33, :] * state + cr[k, 0:32, :]
-        decay = cr[k, 32:40, :] * decay
-    us[0:32, :] = state
-    us[32:40, :] = decay
+        px[k] = state
+        pxd[k] = decay
+        state = crd[k] * state + cr[k]
+        decay = crd[k] * decay
+    us[...] = state
+    usd[...] = decay
     for dz in (4, 3, 5, 2, 6, 1, 7):
-        remote(us, zr.at[z], s_sem.at[3], c_sem.at[2], {"sp_0": (z + dz) % NZ}).start()
+        device = {"sp_0": (z + dz) % NZ}
+        remote(us, zr.at[z], s_sem.at[3], c_sem.at[2], device).start()
+        remote(usd, zrd.at[z], s_sem.at[11], c_sem.at[4], device).start()
     zr[z] = us[...]
+    zrd[z] = usd[...]
     take(zr.at[pl.ds(0, NZ - 1)], c_sem.at[2])
+    take(zrd.at[pl.ds(0, NZ - 1)], c_sem.at[4])
     state = jnp.zeros((32, 128), f32)
     for k in range(NZ):
         counts = (k < z).astype(f32)
-        state = (1.0 - counts) * state + counts * (zr[k, 32:33, :] * state + zr[k, 0:32, :])
+        state = (1.0 - counts) * state + counts * (zrd[k] * state + zr[k])
     for k in range(NX * NC):
-        isend[k] = px[k, 32:33, :] * state + px[k, 0:32, :]
+        isend[k] = pxd[k] * state + px[k]
     for dx in (2, 1, 3, 0):
         to = (x + dx) % NX
         for dc in range(NC):
@@ -248,6 +263,7 @@
                     {"sp_1": to, "sp_2": core},
                 ).start()
     inc[c * NX + x] = isend[x * NC + c]
+    down_weights(4)
     take(inc.at[pl.ds(0, NX * NC - 1)], c_sem.at[3])
 
     loads[4].wait()
@@ -283,14 +299,15 @@
     remote(gall.at[down, low], gall.at[down, low], s_sem.at[5], gr.at[0], at_up).start()
     take(gall.at[up, high], gp.at[1])
     remote(gall.at[up, high], gall.at[up, high], s_sem.at[5], gr.at[1], at_down).start()
-    down_weights(2)
-    for n in range(2):
-        rows, other = pl.ds(64 * n, 64), pl.ds(64 * (3 - n), 64)
+    down_weights(5)
+    down_weights(6)
+    for n in range(4):
+        rows, other = pl.ds(32 * n, 32), pl.ds(32 * (7 - n), 32)
         take(wd.at[down, rows], wm.at[n])
         remote(wd.at[down, rows], wd.at[down, rows], s_sem.at[1], wr.at[n], at_up).start()
-        take(wd.at[up, other], wp.at[3 - n])
-        remote(wd.at[up, other], wd.at[up, other], s_sem.at[1], wr.at[3 - n], at_down).start()
-    down_weights(3)
+        take(wd.at[up, other], wp.at[7 - n])
+        remote(wd.at[up, other], wd.at[up, other], s_sem.at[1], wr.at[7 - n], at_down).start()
+    down_weights(7)
     take(gall.at[down, high], gm.at[1])
     project(down, False)
     take(gall.at[up, low], gp.at[0])
@@ -318,35 +335,40 @@
     dest0, dest1 = dest[0:1, :], dest[1:2, :]
     slot = lax.broadcasted_iota(jnp.int32, (128, ROWS), 0)
 
-    def dispatch(n, _):
+    def slots_of(n, quarter):
         ids = (slot + n * 128).astype(f32)
         pick = jnp.where((ids == dest0) | (ids == dest1), 1.0, 0.0).astype(bf16)
-        rows = dot(pick, normed[p]).astype(bf16).reshape(8, 16, 512)
-        sbuf[pl.ds(n * 8, 8)] = rows
+        return dot(pick, normed[quarter]).astype(bf16).reshape(8, 16, 512)
+
+    def dispatch(n, _):
+        sbuf[pl.ds(n * 8, 8)] = slots_of(n, p)
         dz = ring_step(n)
         for j in range(8):
-            device = {
-                "sp_0": (z + dz) % NZ, "sp_1": (x + j // 2) % NX, "sp_2": (c + j % 2) % NC,
-            }
-
-            def send(j=j, device=device):
-                remote(
-                    sbuf.at[n * 8 + j], xbuf.at[p, n * 8 + j], s_sem.at[6], xs.at[n], device
-                ).start()
-
-            if j:
-                send()
-            else:
-                pl.when(n > 0)(send)
-
-                @pl.when(n == 0)
-                def _():
-                    xbuf[p, 0] = rows[0]
-
-
+            remote(
+                sbuf.at[n * 8 + j], xbuf.at[p, n * 8 + j], s_sem.at[6], xs.at[n],
+                {"sp_0": (z + dz) % NZ, "sp_1": (x + j // 2) % NX, "sp_2": (c + j % 2) % NC},
+            ).start()
         return 0
 
-    lax.fori_loop(0, NZ, dispatch, 0)
+    lax.fori_loop(1, NZ, dispatch, 0)
+    def direct(k, n, quarter, sem):
+        rows = slots_of(n, quarter)
+        sdir[k] = rows
+        for j in range(n == 0, 8):
+            remote(
+                sdir.at[k, j], xbuf.at[quarter, n * 8 + j], s_sem.at[0], sem,
+                {
+                    "sp_0": (z + ORDER[n]) % NZ,
+                    "sp_1": (x + j // 2) % NX,
+                    "sp_2": (c + j % 2) % NC,
+                },
+            ).start()
+        return rows
+
+    for quarter in range(NY):
+        xbuf[quarter, 0] = direct(quarter, 0, quarter, xs.at[0])[0]
+    for n in range(NEAR, NZ):
+        direct(NY + n - NEAR, n, far, yrm.at[n])
     loads[7].wait()
     loads[8].wait()
 
@@ -358,29 +380,41 @@
     def stage_forward(n):
         group = pl.ds(n * 8, 8)
 
-        @pl.when(n == 0)
-        def _():
-            take(xbuf.at[p, pl.ds(1, 7)], xs.at[n])
-
-        @pl.when(n > 0)
-        def _():
-            take(xbuf.at[p, group], xs.at[n])
-
+        take(xbuf.at[p, group], xs.at[n])
         remote(xbuf.at[p, group], xbuf.at[p, group], s_sem.at[7], yfm.at[n], at_up).start()
         remote(xbuf.at[p, group], xbuf.at[p, group], s_sem.at[7], yfp.at[n], at_down).start()
 
     def stage_relay(n):
         group = pl.ds(n * 8, 8)
-        front, back = pl.ds(n * 8, 3), pl.ds(n * 8 + 3, 5)
+        front, back = pl.ds(n * 8, 4), pl.ds(n * 8 + 4, 4)
         take(xbuf.at[down, group], yfm.at[n])
-        remote(xbuf.at[down, front], xbuf.at[down, front], s_sem.at[7], yrm.at[n], at_up).start()
+
+        @pl.when(n < NEAR)
+        def _():
+            remote(xbuf.at[down, front], xbuf.at[down, front], s_sem.at[7], yrm.at[n], at_up).start()
+
         take(xbuf.at[up, group], yfp.at[n])
-        remote(xbuf.at[up, back], xbuf.at[up, back], s_sem.at[7], yrp.at[n], at_down).start()
+
+        @pl.when(n < NEAR)
+        def _():
+            remote(xbuf.at[up, back], xbuf.at[up, back], s_sem.at[7], yrp.at[n], at_down).start()
+
 
     def stage_hidden(n):
         group = pl.ds(n * 8, 8)
-        take(xbuf.at[far, pl.ds(n * 8, 3)], yrm.at[n])
-        take(xbuf.at[far, pl.ds(n * 8 + 3, 5)], yrp.at[n])
+        @pl.when(n == 0)
+        def _():
+            take(xbuf.at[0, pl.ds(0, 28)], xs.at[0])
+
+        @pl.when(n >= NEAR)
+        def _():
+            take(xbuf.at[far, group], yrm.at[n])
+
+        @pl.when((n > 0) & (n < NEAR))
+        def _():
+            take(xbuf.at[far, pl.ds(n * 8, 4)], yrm.at[n])
+            take(xbuf.at[far, pl.ds(n * 8 + 4, 4)], yrp.at[n])
+
         rows = jnp.concatenate([xbuf[k, group].reshape(128, 512) for k in range(NY)], axis=1)
         gate = dot(rows, wg[...])
         hidden = (gate * jax.nn.sigmoid(gate) * dot(rows, wu[...])).astype(bf16)
@@ -423,12 +457,13 @@
                     rbuf[0] = outs[0]
 
 
-    def pipeline(i, _):
+    @pl.loop(1, NZ + 3)
+    def _(i):
         @pl.when(i < NZ)
         def _():
             stage_forward(i)
 
-        @pl.when((i >= 1) & (i < NZ + 1))
+        @pl.when((i >= 2) & (i < NZ + 1))
         def _():
             stage_relay(i - 1)
 
@@ -438,19 +473,15 @@
 
         @pl.when(i == 3)
         def _():
-            for n in range(2):
-                take(wd.at[down, pl.ds(64 * (n + 2), 64)], wm.at[n + 2])
-                take(wd.at[up, pl.ds(64 * n, 64)], wp.at[n])
             for n in range(4):
-                take(wd.at[far, pl.ds(64 * n, 64)], wr.at[n])
+                take(wd.at[down, pl.ds(32 * (n + 4), 32)], wm.at[n + 4])
+                take(wd.at[up, pl.ds(32 * n, 32)], wp.at[n])
+            for n in range(8):
+                take(wd.at[far, pl.ds(32 * n, 32)], wr.at[n])
 
         @pl.when(i >= 3)
         def _():
             stage_down(i - 3)
-
-        return 0
-
-    lax.fori_loop(0, NZ + 3, pipeline, 0)
 
     picks[...] = jnp.zeros_like(picks)
     own_rows = pl.ds(pl.multiple_of(p * GROUP, GROUP), GROUP)
@@ -483,11 +514,17 @@
 
     take(wd.at[pl.ds(0, 3)], s_sem.at[1])
     take(cr.at[pl.ds(0, 7)], s_sem.at[2])
+    take(crd.at[pl.ds(0, 7)], s_sem.at[10])
     take(zr.at[pl.ds(0, 7)], s_sem.at[3])
+    take(zrd.at[pl.ds(0, 7)], s_sem.at[11])
     take(inc.at[pl.ds(0, 7)], s_sem.at[4])
     take(gall.at[pl.ds(0, 3)], s_sem.at[5])
-    take(sbuf.at[pl.ds(0, 63)], s_sem.at[6])
-    take(xbuf.at[pl.ds(0, 3)], s_sem.at[7])
+    take(xbuf.at[0, pl.ds(0, 28)], s_sem.at[0])
+    take(xbuf.at[0, pl.ds(0, 8 * (NZ - NEAR))], s_sem.at[0])
+    take(sbuf.at[pl.ds(0, 56)], s_sem.at[6])
+    for k in range(2):
+        take(xbuf.at[k, pl.ds(0, 8 * (NZ - 1))], s_sem.at[7])
+    take(xbuf.at[2, pl.ds(0, 8 * (NEAR - 1))], s_sem.at[7])
     take(hrec.at[pl.ds(0, 6)], s_sem.at[8])
     take(rbuf.at[pl.ds(0, 63)], s_sem.at[9])
 
@@ -512,15 +549,16 @@
             V((ROWS, 256), bf16), V((ROWS, 256), bf16), V((ROWS, 256), bf16), V((ROWS, 256), bf16),
             V((ROWS, 2048), bf16), V((4, 256, 2048), bf16), V((2048, 256), bf16),
             V((2048, 256), bf16), V((4, 256, 2048), bf16),
-            V((2, ROWS, 128), f32), V((ROWS, 256), f32), V((8, 40, 128), f32), V((8, 40, 128), f32),
-            V((8, 40, 128), f32), V((40, 128), f32), V((8, 40, 128), f32), V((8, 32, 128), f32),
-            V((8, 32, 128), f32), V((2, ROWS), f32), V((2, ROWS, 128), f32),
+            V((2, ROWS, 128), f32), V((ROWS, 256), f32), V((8, 32, 128), f32), V((8, 1, 128), f32),
+            V((8, 32, 128), f32), V((8, 1, 128), f32), V((8, 32, 128), f32), V((8, 1, 128), f32),
+            V((32, 128), f32), V((1, 128), f32), V((8, 32, 128), f32), V((8, 1, 128), f32),
+            V((8, 32, 128), f32), V((8, 32, 128), f32), V((2, ROWS), f32), V((2, ROWS, 128), f32),
             V((4, ROWS, 256), bf16), V((ROWS, 2048), f32), V((ROWS, 2048), bf16),
             V((4, ROWS, 512), bf16), V((64, 16, 512), bf16), V((4, 64, 16, 512), bf16),
             V((8, 4, 32, 256), bf16), V((8, 4, 32, 256), bf16), V((64, 16, 512), bf16),
-            V((64, 16, 512), bf16), V((4, 128, 512), f32),
-            dma((9,)), dma((10,)), dma((4,)), dma((2,)), dma((2,)), dma((2,)), dma((4,)), dma((4,)),
-            dma((4,)), dma((8,)), dma((8,)), dma((8,)), dma((8,)), dma((8,)), dma((8,)), dma((8,)),
+            V((64, 16, 512), bf16), V((4, 128, 512), f32), V((6, 8, 16, 512), bf16),
+            dma((9,)), dma((12,)), dma((5,)), dma((2,)), dma((2,)), dma((2,)), dma((8,)), dma((8,)),
+            dma((8,)), dma((8,)), dma((8,)), dma((8,)), dma((8,)), dma((8,)), dma((8,)), dma((8,)),
         ],
         compiler_params=pltpu.CompilerParams(
             collective_id=0, has_side_effects=True, vmem_limit_bytes=60 * 1024 * 1024

time: 115 us -> 103 us (0.90)
  Pallas kernels: 113 us -> 102 us
    pallas_call x1, Pallas kernels: 113 us -> 102 us  [per_device(): pl.pallas_call(kernel, name='layer', out_shape=jax.ShapeDtypeStruct((GROU...]
where the time goes in v3:
time: 103 us
  Pallas kernels  102 us (99%)
  local copies, waits for them, and re-layouts  1.67 us (2%)
    pallas_call x1, Pallas kernels, per_device(): pl.pallas_call(kernel, name='layer', out_shape=jax.ShapeDtypeStruct((GROU...  102 us

profile of v3, /device:TPU:1, one launch (start us, length us, event | category | flops | bytes accessed | tf_op | source)
XLA Modules:
  0.0 103.3 jit_solution(11525592649822657764)
XLA Ops:
  0.0 101.6 %layer.1 = bf16[64,2048]{1,0:T(8,128)(2,1)} custom-call(s32[2,256]{1,0:T(2,128)} %bitcast.14, f32[2,64]{1,0:T(2,128)} %bitcast.16, f32[2,128]{1,0:T(2,128)} %mar_ref.1, f32[2,256]{1,0:T(2,128)} %bitcast.15, f32[1,128]{1,0:T(1,128)} %bitcast.17, f32[1,2048]{1,0:T(1,128)} %bitcast.13, bf16[256,256]{1,0:T(8,128)(2,1)} %q_hbm.1, bf16[256,256]{1,0:T(8,128)(2,1)} %f_hbm.1, ...), custom_call_target="tpu_custom_call" | custom-call | tf_op jit(solution)/shard_map/layer/pallas_call | solution.py:542
  101.6 1.7 %copy.17 = bf16[64,2048]{1,0:T(8,128)(2,1)} copy(bf16[64,2048]{1,0:T(8,128)(2,1)} %layer.1) | data formatting | bytes 524288

commit v4 on v3

--- a/solution.py
+++ b/solution.py
@@ -47,7 +47,7 @@
 
 
 ORDER = (0, 4, 3, 5, 6, 2, 7, 1)
-NEAR = 6
+NEAR = 4
 PACKED = sum(dz << (3 * n) for n, dz in enumerate(ORDER))
 
 
@@ -77,7 +77,7 @@
     qb, fb, vb, ob, stream, wh, wg, wu, wd,
     rec, qend, cs, csd, cr, crd, px, pxd, us, usd, zr, zrd, isend, inc, dest, dcol,
     gall, acc, mixed, normed, sbuf, xbuf, hsend, hrec, rsend, rbuf, picks, sdir,
-    load_sem, s_sem, c_sem, gm, gp, gr, wm, wp, wr, xs, yfm, yfp, yrm, yrp, hs, rs,
+    load_sem, s_sem, c_sem, g_sem, wm, wp, wr, xs, yfm, yfp, yrm, yrp, hs, rs,
 ):
     z, x, c, p = [lax.axis_index(name) for name in SP_TP]
     up, down, far = (p + 1) % NY, (p + NY - 1) % NY, (p + 2) % NY
@@ -276,12 +276,10 @@
         gated = recur * scale * hg_ref[...] * (gate_in * jax.nn.sigmoid(gate_in))
         gall[p, :, lanes] = gated.astype(bf16)
 
-    for half in range(2):
-        rows = pl.ds(128 * half, 128)
-        other = pl.ds(128 * (1 - half), 128)
-        remote(gall.at[p, rows], gall.at[p, rows], s_sem.at[5], gm.at[half], at_up).start()
-        remote(gall.at[p, other], gall.at[p, other], s_sem.at[5], gp.at[1 - half], at_down).start()
-    low, high = pl.ds(0, 128), pl.ds(128, 128)
+    for k, peer in enumerate((up, down, far)):
+        remote(gall.at[p], gall.at[p], s_sem.at[5], g_sem.at[k], {"tp": peer}).start()
+    for n in range(5, 8):
+        down_weights(n)
     loads[5].wait()
 
     def project(source, fresh):
@@ -295,25 +293,17 @@
                 acc[:, cols] = acc[:, cols] + part
 
     project(p, True)
-    take(gall.at[down, low], gm.at[0])
-    remote(gall.at[down, low], gall.at[down, low], s_sem.at[5], gr.at[0], at_up).start()
-    take(gall.at[up, high], gp.at[1])
-    remote(gall.at[up, high], gall.at[up, high], s_sem.at[5], gr.at[1], at_down).start()
-    down_weights(5)
-    down_weights(6)
+    take(gall.at[down], g_sem.at[0])
     for n in range(4):
         rows, other = pl.ds(32 * n, 32), pl.ds(32 * (7 - n), 32)
         take(wd.at[down, rows], wm.at[n])
         remote(wd.at[down, rows], wd.at[down, rows], s_sem.at[1], wr.at[n], at_up).start()
         take(wd.at[up, other], wp.at[7 - n])
         remote(wd.at[up, other], wd.at[up, other], s_sem.at[1], wr.at[7 - n], at_down).start()
-    down_weights(7)
-    take(gall.at[down, high], gm.at[1])
     project(down, False)
-    take(gall.at[up, low], gp.at[0])
+    take(gall.at[up], g_sem.at[1])
     project(up, False)
-    take(gall.at[far, low], gr.at[0])
-    take(gall.at[far, high], gr.at[1])
+    take(gall.at[far], g_sem.at[2])
     project(far, False)
 
     loads[6].wait()
@@ -457,19 +447,29 @@
                     rbuf[0] = outs[0]
 
 
-    @pl.loop(1, NZ + 3)
+    stage_forward(1)
+    stage_hidden(0)
+    stage_relay(1)
+    stage_forward(2)
+    stage_hidden(1)
+
+    @pl.loop(3, NZ + 2)
     def _(i):
         @pl.when(i < NZ)
         def _():
             stage_forward(i)
 
-        @pl.when((i >= 2) & (i < NZ + 1))
+        @pl.when(i < NZ + 1)
         def _():
             stage_relay(i - 1)
 
-        @pl.when((i >= 2) & (i < NZ + 2))
+        @pl.when((i >= 4) & (i <= NEAR + 1))
         def _():
             stage_hidden(i - 2)
+
+        @pl.when((i >= NEAR + 1) & (i < NZ + 1))
+        def _():
+            stage_hidden(i - 1)
 
         @pl.when(i == 3)
         def _():
@@ -478,10 +478,16 @@
                 take(wd.at[up, pl.ds(32 * n, 32)], wp.at[n])
             for n in range(8):
                 take(wd.at[far, pl.ds(32 * n, 32)], wr.at[n])
-
-        @pl.when(i >= 3)
+            stage_down(0)
+            stage_down(1)
+
+        @pl.when((i == NEAR + 1) | (i == NEAR + 2))
         def _():
             stage_down(i - 3)
+
+        @pl.when(i >= NEAR + 2)
+        def _():
+            stage_down(i - 2)
 
     picks[...] = jnp.zeros_like(picks)
     own_rows = pl.ds(pl.multiple_of(p * GROUP, GROUP), GROUP)
@@ -556,8 +562,8 @@
             V((4, ROWS, 256), bf16), V((ROWS, 2048), f32), V((ROWS, 2048), bf16),
             V((4, ROWS, 512), bf16), V((64, 16, 512), bf16), V((4, 64, 16, 512), bf16),
             V((8, 4, 32, 256), bf16), V((8, 4, 32, 256), bf16), V((64, 16, 512), bf16),
-            V((64, 16, 512), bf16), V((4, 128, 512), f32), V((6, 8, 16, 512), bf16),
-            dma((9,)), dma((12,)), dma((5,)), dma((2,)), dma((2,)), dma((2,)), dma((8,)), dma((8,)),
+            V((64, 16, 512), bf16), V((4, 128, 512), f32), V((8, 8, 16, 512), bf16),
+            dma((9,)), dma((12,)), dma((5,)), dma((3,)), dma((8,)), dma((8,)),
             dma((8,)), dma((8,)), dma((8,)), dma((8,)), dma((8,)), dma((8,)), dma((8,)), dma((8,)),
         ],
         compiler_params=pltpu.CompilerParams(

time: 103 us -> 101 us (0.981)
  Pallas kernels: 102 us -> 99.6 us
    pallas_call x1, Pallas kernels: 102 us -> 99.6 us  [per_device(): pl.pallas_call(kernel, name='layer', out_shape=jax.ShapeDtypeStruct((GROU...]
where the time goes in v4:
time: 101 us
  Pallas kernels  99.6 us (99%)
  local copies, waits for them, and re-layouts  1.67 us (2%)
    pallas_call x1, Pallas kernels, per_device(): pl.pallas_call(kernel, name='layer', out_shape=jax.ShapeDtypeStruct((GROU...  99.6 us

profile of v4, /device:TPU:1, one launch (start us, length us, event | category | flops | bytes accessed | tf_op | source)
XLA Modules:
  0.0 101.3 jit_solution(7478375256352098296)
XLA Ops:
  0.0 99.6 %layer.1 = bf16[64,2048]{1,0:T(8,128)(2,1)} custom-call(s32[2,256]{1,0:T(2,128)} %bitcast.14, f32[2,64]{1,0:T(2,128)} %bitcast.16, f32[2,128]{1,0:T(2,128)} %mar_ref.1, f32[2,256]{1,0:T(2,128)} %bitcast.15, f32[1,128]{1,0:T(1,128)} %bitcast.17, f32[1,2048]{1,0:T(1,128)} %bitcast.13, bf16[256,256]{1,0:T(8,128)(2,1)} %q_hbm.1, bf16[256,256]{1,0:T(8,128)(2,1)} %f_hbm.1, ...), custom_call_target="tpu_custom_call" | custom-call | tf_op jit(solution)/shard_map/layer/pallas_call | solution.py:548
  99.6 1.7 %copy.17 = bf16[64,2048]{1,0:T(8,128)(2,1)} copy(bf16[64,2048]{1,0:T(8,128)(2,1)} %layer.1) | data formatting | bytes 524288

commit v5 on v3

--- a/solution.py
+++ b/solution.py
@@ -47,7 +47,7 @@
 
 
 ORDER = (0, 4, 3, 5, 6, 2, 7, 1)
-NEAR = 6
+NEAR = 4
 PACKED = sum(dz << (3 * n) for n, dz in enumerate(ORDER))
 
 
@@ -457,19 +457,29 @@
                     rbuf[0] = outs[0]
 
 
-    @pl.loop(1, NZ + 3)
+    stage_forward(1)
+    stage_hidden(0)
+    stage_relay(1)
+    stage_forward(2)
+    stage_hidden(1)
+
+    @pl.loop(3, NZ + 2)
     def _(i):
         @pl.when(i < NZ)
         def _():
             stage_forward(i)
 
-        @pl.when((i >= 2) & (i < NZ + 1))
+        @pl.when(i < NZ + 1)
         def _():
             stage_relay(i - 1)
 
-        @pl.when((i >= 2) & (i < NZ + 2))
+        @pl.when((i >= 4) & (i <= NEAR + 1))
         def _():
             stage_hidden(i - 2)
+
+        @pl.when((i >= NEAR + 1) & (i < NZ + 1))
+        def _():
+            stage_hidden(i - 1)
 
         @pl.when(i == 3)
         def _():
@@ -478,10 +488,16 @@
                 take(wd.at[up, pl.ds(32 * n, 32)], wp.at[n])
             for n in range(8):
                 take(wd.at[far, pl.ds(32 * n, 32)], wr.at[n])
-
-        @pl.when(i >= 3)
+            stage_down(0)
+            stage_down(1)
+
+        @pl.when((i == NEAR + 1) | (i == NEAR + 2))
         def _():
             stage_down(i - 3)
+
+        @pl.when(i >= NEAR + 2)
+        def _():
+            stage_down(i - 2)
 
     picks[...] = jnp.zeros_like(picks)
     own_rows = pl.ds(pl.multiple_of(p * GROUP, GROUP), GROUP)
@@ -556,7 +572,7 @@
             V((4, ROWS, 256), bf16), V((ROWS, 2048), f32), V((ROWS, 2048), bf16),
             V((4, ROWS, 512), bf16), V((64, 16, 512), bf16), V((4, 64, 16, 512), bf16),
             V((8, 4, 32, 256), bf16), V((8, 4, 32, 256), bf16), V((64, 16, 512), bf16),
-            V((64, 16, 512), bf16), V((4, 128, 512), f32), V((6, 8, 16, 512), bf16),
+            V((64, 16, 512), bf16), V((4, 128, 512), f32), V((8, 8, 16, 512), bf16),
             dma((9,)), dma((12,)), dma((5,)), dma((2,)), dma((2,)), dma((2,)), dma((8,)), dma((8,)),
             dma((8,)), dma((8,)), dma((8,)), dma((8,)), dma((8,)), dma((8,)), dma((8,)), dma((8,)),
         ],

time: 103 us -> 102 us (level)
  Pallas kernels: 102 us -> 99.7 us
    pallas_call x1, Pallas kernels: 102 us -> 99.7 us  [per_device(): pl.pallas_call(kernel, name='layer', out_shape=jax.ShapeDtypeStruct((GROU...]
where the time goes in v5:
time: 102 us; the launch traced here: 101 us
  Pallas kernels  99.7 us (98%)
  local copies, waits for them, and re-layouts  1.67 us (2%)
    pallas_call x1, Pallas kernels, per_device(): pl.pallas_call(kernel, name='layer', out_shape=jax.ShapeDtypeStruct((GROU...  99.7 us

profile of v5, /device:TPU:1, one launch (start us, length us, event | category | flops | bytes accessed | tf_op | source)
XLA Modules:
  0.0 101.4 jit_solution(8208273237594111808)
XLA Ops:
  0.0 99.7 %layer.1 = bf16[64,2048]{1,0:T(8,128)(2,1)} custom-call(s32[2,256]{1,0:T(2,128)} %bitcast.14, f32[2,64]{1,0:T(2,128)} %bitcast.16, f32[2,128]{1,0:T(2,128)} %mar_ref.1, f32[2,256]{1,0:T(2,128)} %bitcast.15, f32[1,128]{1,0:T(1,128)} %bitcast.17, f32[1,2048]{1,0:T(1,128)} %bitcast.13, bf16[256,256]{1,0:T(8,128)(2,1)} %q_hbm.1, bf16[256,256]{1,0:T(8,128)(2,1)} %f_hbm.1, ...), custom_call_target="tpu_custom_call" | custom-call | tf_op jit(solution)/shard_map/layer/pallas_call | solution.py:558
  99.7 1.7 %copy.17 = bf16[64,2048]{1,0:T(8,128)(2,1)} copy(bf16[64,2048]{1,0:T(8,128)(2,1)} %layer.1) | data formatting | bytes 524288

commit v6 on v5

--- a/solution.py
+++ b/solution.py
@@ -47,7 +47,7 @@
 
 
 ORDER = (0, 4, 3, 5, 6, 2, 7, 1)
-NEAR = 4
+NEAR = 6
 PACKED = sum(dz << (3 * n) for n, dz in enumerate(ORDER))
 
 
@@ -491,7 +491,7 @@
             stage_down(0)
             stage_down(1)
 
-        @pl.when((i == NEAR + 1) | (i == NEAR + 2))
+        @pl.when((i >= 5) & (i <= NEAR + 2))
         def _():
             stage_down(i - 3)
 

time: 102 us -> 102 us (level)
  Pallas kernels: 99.7 us -> 101 us
where the time goes in v6:
time: 102 us
  Pallas kernels  101 us (99%)
  local copies, waits for them, and re-layouts  1.67 us (2%)
    pallas_call x1, Pallas kernels, per_device(): pl.pallas_call(kernel, name='layer', out_shape=jax.ShapeDtypeStruct((GROU...  101 us

profile of v6, /device:TPU:1, one launch (start us, length us, event | category | flops | bytes accessed | tf_op | source)
XLA Modules:
  0.0 102.3 jit_solution(14518478464605376962)
XLA Ops:
  0.0 100.6 %layer.1 = bf16[64,2048]{1,0:T(8,128)(2,1)} custom-call(s32[2,256]{1,0:T(2,128)} %bitcast.14, f32[2,64]{1,0:T(2,128)} %bitcast.16, f32[2,128]{1,0:T(2,128)} %mar_ref.1, f32[2,256]{1,0:T(2,128)} %bitcast.15, f32[1,128]{1,0:T(1,128)} %bitcast.17, f32[1,2048]{1,0:T(1,128)} %bitcast.13, bf16[256,256]{1,0:T(8,128)(2,1)} %q_hbm.1, bf16[256,256]{1,0:T(8,128)(2,1)} %f_hbm.1, ...), custom_call_target="tpu_custom_call" | custom-call | tf_op jit(solution)/shard_map/layer/pallas_call | solution.py:558
  100.6 1.7 %copy.17 = bf16[64,2048]{1,0:T(8,128)(2,1)} copy(bf16[64,2048]{1,0:T(8,128)(2,1)} %layer.1) | data formatting | bytes 524288
